TPU v7x, 32 devices: a whole 2x2x4 slice. The times are simulated.
32 devices in a mesh: sp: 16 (over z, y, core), tp: 2 (over x).
Axes of the slice: x: 2, y: 2, z: 4, core: 2. Of those that a mesh axis runs over, the one named last changes fastest.
Arguments:
- tokens: bfloat16 [6144, 2048], P('sp', 'tp'), may hold values from -60 to 60
- pre_gain: bfloat16 [2048], P('tp'), may hold values from 0.099609375 to 1.8984375
- w_query: bfloat16 [2048, 1024], P('sp', 'tp'), may hold values from -1 to 1
- w_key: bfloat16 [2048, 1024], P('sp', 'tp'), may hold values from -1 to 1
- w_value: bfloat16 [2048, 1024], P('sp', 'tp'), may hold values from -0.125 to 0.125
- w_pool: bfloat16 [2048, 1024], P('sp', 'tp'), may hold values from -0.125 to 0.125
- lambdas: float32 [8], P('tp'), may hold values from 0.3 to 0.8
- sub_gain: float32 [128], replicated, may hold values from 0.1 to 1.9
- group_weight: bfloat16 [8, 128, 128], P('tp'), may hold values from -0.5 to 0.5
- pool_scale: float32 [1024], P('tp'), may hold values from 0.1 to 1.9
- w_out: bfloat16 [2048, 2048], P('tp', 'sp'), may hold values from -0.125 to 0.125
Outputs:
- mixed_out: bfloat16 [6144, 2048], P(('sp', 'tp'))
All inputs are finite; a program needn't handle non-finite values.
Results may differ from a plain program's by a relative error of at most 0.015.
Values may be sent and summed in bfloat16 or wider, within the bound.
A program may use at most 128 MiB of HBM per device.

v0:
```python
import math

import jax
import jax.numpy as jnp
from jax import lax
from jax.sharding import PartitionSpec as P

EPSILON = 1e-06
NEG_LARGE = -1e30
WINDOWS = (2, 4, 8, 16)
RIM_ROWS = 15


def passed_along(block, axis, distance):
    devices = range(lax.axis_size(axis))
    route = [(i - distance, i) for i in devices if i - distance in devices]
    return lax.ppermute(block, axis, route)


def unchanged(carried):
    return carried


def local(
    tokens,
    pre_gain,
    w_query,
    w_key,
    w_value,
    w_pool,
    lambdas,
    sub_gain,
    group_weight,
    pool_scale,
    w_out,
):
    tok_rows = tokens.shape[0]
    model_width = tokens.shape[1] * lax.axis_size("tp")
    local_heads = lambdas.shape[0]
    head_dim = w_query.shape[1] // (2 * local_heads)
    value_dim = w_value.shape[1] // local_heads
    local_groups = group_weight.shape[0]
    group_dim = group_weight.shape[1]
    q_cols = w_query.shape[1]
    v_cols = w_value.shape[1]
    w_cat = jnp.concatenate([w_query, w_key, w_value, w_pool], axis=1)
    w_in_full, w_out_rows = (
        lax.all_gather(w_cat, "sp", axis=0, tiled=True),
        lax.all_gather(w_out, "sp", axis=1, tiled=True),
    )
    gain_row = pre_gain.reshape(1, -1)
    pieces = (
        lax.all_gather(tokens, "tp", axis=1, tiled=True),
        lax.all_gather(gain_row, "tp", axis=1, tiled=True),
    )
    feature_part = pieces[0].astype(jnp.float32)
    scaled = (feature_part * pieces[1].astype(jnp.float32)).astype(jnp.bfloat16)
    projection = jnp.dot(scaled, w_in_full, preferred_element_type=jnp.float32)
    projection, squares = (projection, jnp.sum(feature_part * feature_part, axis=1))
    inverse = lax.rsqrt(squares / model_width + EPSILON)
    projected = (projection * inverse[:, None]).astype(jnp.bfloat16)
    queries = projected[:, :q_cols].reshape(tok_rows, local_heads, 2, head_dim)
    key_rows = projected[:, q_cols : 2 * q_cols]
    values = projected[:, 2 * q_cols : 2 * q_cols + v_cols]
    pool_in = projected[:, 2 * q_cols + v_cols :]
    first_row = lax.axis_index("sp") * tok_rows
    positions = first_row + jnp.arange(tok_rows, dtype=jnp.int32)
    shard_group = tok_rows * max(1, 1024 // tok_rows)
    score_scale = 1.0 / math.sqrt(head_dim)
    last_query = first_row + tok_rows - 1
    initial_max = jnp.full((local_heads, 2, tok_rows), NEG_LARGE, jnp.float32)
    initial_sum = jnp.zeros((local_heads, 2, tok_rows), jnp.float32)
    initial_weighted = jnp.zeros((local_heads, 2, tok_rows, value_dim), jnp.float32)
    pieces = (
        lax.all_gather(key_rows, "sp", axis=0, tiled=True),
        lax.all_gather(values, "sp", axis=0, tiled=True),
    )
    key_piece = pieces[0].reshape(-1, local_heads, 2, head_dim)
    value_piece = pieces[1].reshape(-1, local_heads, value_dim)
    length = key_piece.shape[0]
    block_len = math.gcd(length, shard_group)

    def one_block(block_index, state):
        block_start = block_index * block_len

        def compute(inner):
            running_max, running_sum, weighted = inner
            key_block = lax.dynamic_slice_in_dim(key_piece, block_start, block_len, 0)
            value_block = lax.dynamic_slice_in_dim(value_piece, block_start, block_len, 0)
            scores = (
                jnp.einsum(
                    "qhmd,khmd->hmqk", queries, key_block, preferred_element_type=jnp.float32
                )
                * score_scale
            )
            key_pos = block_start + jnp.arange(block_len, dtype=jnp.int32)
            allowed = key_pos[None, :] <= positions[:, None]
            scores = jnp.where(allowed, scores, NEG_LARGE)
            new_max = jnp.maximum(running_max, jnp.max(scores, axis=-1))
            factor = jnp.exp(running_max - new_max)
            expo = jnp.where(allowed, jnp.exp(scores - new_max[..., None]), 0.0)
            running_sum = running_sum * factor + jnp.sum(expo, axis=-1)
            weighted = weighted * factor[..., None] + jnp.einsum(
                "hmqk,khd->hmqd",
                expo.astype(jnp.bfloat16),
                value_block,
                preferred_element_type=jnp.float32,
            )
            return (new_max, running_sum, weighted)

        return lax.cond(block_start <= last_query, compute, unchanged, state)

    running_max, running_sum, weighted = lax.fori_loop(
        0, length // block_len, one_block, (initial_max, initial_sum, initial_weighted)
    )
    head_mix = (
        weighted[:, 0] / running_sum[:, 0, :, None]
        - lambdas[:, None, None] * weighted[:, 1] / running_sum[:, 1, :, None]
    )
    mean_sq = jnp.mean(head_mix * head_mix, axis=-1, keepdims=True)
    normed = head_mix * lax.rsqrt(mean_sq + EPSILON) * sub_gain
    attention = jnp.transpose(normed, (1, 0, 2)).astype(jnp.bfloat16)
    halo_rows = passed_along(pool_in[tok_rows - RIM_ROWS :], "sp", 1)
    extended = jnp.concatenate([halo_rows, pool_in], axis=0).astype(jnp.float32)
    running = jnp.concatenate(
        [jnp.zeros((1, extended.shape[1]), jnp.float32), jnp.cumsum(extended, axis=0)], axis=0
    )
    running_top = running[RIM_ROWS + 1 :]
    window_ids = (
        lax.axis_index("tp") * local_groups + jnp.arange(local_groups, dtype=jnp.int32)
    ) % len(WINDOWS)
    column_window = jnp.repeat(window_ids, group_dim)
    average = jnp.zeros_like(running_top)
    for window_slot, window_span in enumerate(WINDOWS):
        running_low = running[RIM_ROWS + 1 - window_span : RIM_ROWS + 1 - window_span + tok_rows]
        window_count = jnp.minimum(positions + 1, window_span).astype(jnp.float32)
        average = average + jnp.where(
            column_window[None, :] == window_slot,
            (running_top - running_low) / window_count[:, None],
            0.0,
        )
    differ = (
        (average - pool_in.astype(jnp.float32))
        .astype(jnp.bfloat16)
        .reshape(tok_rows, local_groups, group_dim)
    )
    pooled = jnp.einsum("tgc,gcd->tgd", differ, group_weight, preferred_element_type=jnp.float32)
    pooled = (pooled * pool_scale.reshape(local_groups, group_dim)).astype(jnp.bfloat16)
    branch = jnp.concatenate([attention, pooled], axis=2).reshape(tok_rows, -1)
    return lax.psum_scatter(
        jnp.dot(branch, w_out_rows, preferred_element_type=jnp.float32).astype(jnp.bfloat16),
        "tp",
        scatter_dimension=0,
        tiled=True,
    )


def solution(mesh):
    placed = (
        P("sp", "tp"),
        P("tp"),
        P("sp", "tp"),
        P("sp", "tp"),
        P("sp", "tp"),
        P("sp", "tp"),
        P("tp"),
        P(),
        P("tp", None, None),
        P("tp"),
        P("tp", "sp"),
    )
    return jax.shard_map(
        local, mesh=mesh, in_specs=placed, out_specs=P(("sp", "tp"), None), check_vma=False
    )
```

profile of v0, /device:TPU:0, one launch (start us, length us, event | category | flops | bytes accessed | tf_op | source)
XLA Modules:
  0.0 377.3 jit_solution(12847883650176811688)
XLA Ops:
  6.5 0.0 copy-start
  6.5 0.0 all-gather.7.cloned.1.call-start
  6.5 0.7 all-gather.7.cloned.1.call-update
  7.3 0.0 all-gather.9.cloned.1.call-start
  7.3 1.9 pad_maximum_fusion.1
  9.2 0.0 all-gather.9.cloned.1.call-update
  9.3 0.0 all-gather.11.cloned.1.call-start
  9.3 5.5 %all-gather = bf16[2048]{0:T(1024)(128)(2,1)S(1)} all-gather(bf16[1024]{0:T(1024)(128)(2,1)} %param.16), channel_id=2, replica_groups=mesh['sp'=16,'tp'=2] {'tp'}, dimensions={0}, use_global_device_ids=true | all-gather | bytes 6144 | tf_op jit(solution)/shard_map/all_gather | solution.py:54
  14.8 24.0 %all-gather.7.cloned.1.call-done = bf16[384,2048]{1,0:T(8,128)(2,1)} async-done(((bf16[384,1024]{1,0:T(8,128)(2,1)}), bf16[384,2048]{1,0:T(8,128)(2,1)}) %all-gather.7.cloned.1.call-update) | async-done | bytes 1572880 | tf_op jit(solution)/shard_map/all_gather | solution.py:53
  38.8 1.8 fusion.20
  40.6 74.7 %all-gather.9.cloned.1.call-done = bf16[2048,2048]{1,0:T(8,128)(2,1)} async-done(((bf16[128,2048]{1,0:T(8,128)(2,1)}), bf16[2048,2048]{1,0:T(8,128)(2,1)}) %all-gather.9.cloned.1.call-update) | async-done | bytes 8388624 | tf_op jit(solution)/shard_map/all_gather | solution.py:48
  115.3 7.3 %multiply_convert_fusion = bf16[384,2048]{1,0:T(8,128)(2,1)S(1)} fusion(bf16[2048,2048]{1,0:T(8,128)(2,1)} %all-gather.9.cloned.1.call-done, bf16[384,2048]{1,0:T(8,128)(2,1)} %all-gather.7.cloned.1.call-done, f32[2048]{0:T(1024)S(1)} %mul.112, f32[384]{0:T(512)S(1)} %add_rsqrt_fusion.1), kind=kOutput, calls=%fused_computation.28 | convolution fusion | flops 3225157632 | bytes 11544064 | tf_op jit(solution)/shard_map/dot_general | solution.py:58
  122.6 1.0 fusion.51
  123.6 0.0 all-gather.11.cloned.1.call-update
  123.6 0.0 all-gather.13.cloned.1.call-start
  123.7 0.5 all-gather.13.cloned.1.call-update
  124.2 0.0 all-gather.15.cloned.1.call-start
  124.3 0.5 all-gather.15.cloned.1.call-update
  124.8 0.0 reduce-scatter.2.cloned.1.call-start
  124.9 0.1 broadcast_bitcast_fusion
  125.0 0.1 broadcast_bitcast_fusion.1
  125.1 0.1 broadcast_bitcast_fusion.2
  125.1 0.1 broadcast_bitcast_fusion.3
  125.2 2.1 collective-permute-start
  127.4 0.2 copy.34
  127.6 0.6 collective-permute-done
  128.2 0.1 maximum_bitcast_fusion
  128.3 0.1 convert.9
  128.5 0.0 copy-start.4
  128.5 0.7 fusion.25
  129.2 0.1 broadcast_add_fusion.1
  129.3 0.3 copy.39
  129.7 0.1 slice.86
  129.7 0.0 copy-done
  129.7 0.0 copy-done.4
  129.7 1.7 fusion.24
  131.5 52.3 %all-gather.11.cloned.1.call-done = bf16[6144,512]{1,0:T(8,128)(2,1)} async-done(((bf16[384,512]{1,0:T(8,128)(2,1)}), bf16[6144,512]{1,0:T(8,128)(2,1)}) %all-gather.11.cloned.1.call-update) | async-done | bytes 6291472 | tf_op jit(solution)/shard_map/all_gather | solution.py:75
  183.8 8.7 %copy.33 = bf16[6144,512]{0,1:T(8,128)(2,1)} copy(bf16[6144,512]{1,0:T(8,128)(2,1)} %all-gather.11.cloned.1.call-done) | data formatting | bytes 12582912 | tf_op jit(solution)/shard_map/all_gather | solution.py:75
  192.5 53.6 %all-gather.13.cloned.1.call-done = bf16[6144,512]{1,0:T(8,128)(2,1)} async-done(((bf16[384,512]{1,0:T(8,128)(2,1)}), bf16[6144,512]{1,0:T(8,128)(2,1)}) %all-gather.13.cloned.1.call-update) | async-done | bytes 6291472 | tf_op jit(solution)/shard_map/all_gather | solution.py:76
  246.0 6.5 %copy_bitcast_fusion = bf16[6144,4,128]{2,0,1:T(8,128)(2,1)} fusion(bf16[6144,512]{1,0:T(8,128)(2,1)} %all-gather.13.cloned.1.call-done), kind=kLoop, calls=%fused_computation.23 | loop fusion | bytes 12582912
  252.6 0.1 broadcast_in_dim.75
  252.7 0.0 copy-start.2
  252.7 11.3 %while.18 = (s32[]{:T(128)}, f32[4,2,384]{2,1,0:T(2,128)S(1)}, f32[4,2,384]{2,1,0:T(2,128)S(1)}, f32[4,2,384,128]{3,2,1,0:T(8,128)S(1)}, s32[]{:T(128)}, /*index...) while((s32[]{:T(128)}, f32[4,2,384]{2,1,0:T(2,128)S(1)}, ...), condition=%wide.region_6.7_spmd.clone, body=%wide.region_1.6_spmd.clone.sunk | while | flops 937729152 | bytes 34812224 | solution.py:113
  252.7 10.6 %conditional.3 = ((f32[4,2,384]{2,1,0:T(2,128)S(1)}, f32[4,2,384]{2,1,0:T(2,128)S(1)}, f32[4,2,384,128]{3,2,1,0:T(8,128)S(1)})) conditional(s32[]{:T(128)} %convert_element_type.123, (f32[4,2,384]{2,1,0:T(2,128)S(1)}, f32[4,2,384]{2,1,0:T(2,128)S(1)}, f32[4,2,384,128]{3,2,1,0:T(8,128)S(1)}) %tuple.58, (s32[]{:T(128)}, s32[]{:T(128)}, ...), branch_computations={%region_2.0_spmd, %region_3.5_spmd} | conditional | flops 937729152 | bytes 34810448 | solution.py:111
  252.7 0.2 broadcast_compare_fusion
  253.0 2.8 fusion.2
  255.8 2.3 fusion.4
  258.1 5.2 %multiply_add_fusion = f32[4,2,384,128]{3,2,1,0:T(8,128)S(1)} fusion(f32[4,2,384,128]{3,2,1,0:T(8,128)S(1)} %get-tuple-element.182, f32[4,2,768,384]{3,2,1,0:T(8,128)S(1)} %get-tuple-element.278, f32[4,2,384]{2,1,0:T(2,128)S(1)} %max.2, pred[384,768]{0,1:T(8,128)(4,1)S(1)} %broadcast_compare_fusion, bf16[6144,4,128]{2,0,1:T(8,128)(2,1)} %get-tuple-element.183, ...), kind=kOutput, calls=%fused_computation.8 | convolution fusion | flops 616562688 | bytes 13688836 | tf_op jit(solution)/shard_map/while/body/eval_jaxpr/cond/branch_1_fun/hmqk,khd->hmqd/dot_general | solution.py:103
  264.0 0.0 copy-start.3
  264.0 0.5 copy.36
  264.5 0.0 copy-done.2
  264.5 0.2 multiply_reduce_fusion
  264.8 0.0 copy-done.3
  264.8 0.1 fusion.45
  264.9 1.1 pad_maximum_fusion
  266.0 33.3 %all-gather.15.cloned.1.call-done = bf16[1024,2048]{1,0:T(8,128)(2,1)} async-done(((bf16[1024,128]{1,0:T(8,128)(2,1)}), bf16[1024,2048]{1,0:T(8,128)(2,1)}) %all-gather.15.cloned.1.call-update) | async-done | bytes 4194320 | tf_op jit(solution)/shard_map/all_gather | solution.py:49
  299.3 0.0 copy-start.1
  299.3 5.2 %convolution_convert_fusion = bf16[384,2048]{1,0:T(8,128)(2,1)} fusion(bf16[384,1024]{0,1:T(8,128)(2,1)S(1)} %bitcast.99, bf16[1024,2048]{1,0:T(8,128)(2,1)} %all-gather.15.cloned.1.call-done), kind=kOutput, calls=%fused_computation.29 | convolution fusion | flops 1611399168 | bytes 6553600 | tf_op jit(solution)/shard_map/dot_general | solution.py:151
  304.5 0.0 reduce-scatter.2.cloned.1.call-update
  304.5 66.0 %reduce-scatter.2.cloned.1.call-done = bf16[192,2048]{1,0:T(8,128)(2,1)} async-done(((bf16[384,2048]{1,0:T(8,128)(2,1)}), bf16[192,2048]{1,0:T(8,128)(2,1)}) %reduce-scatter.2.cloned.1.call-update) | async-done | bytes 786448 | tf_op jit(solution)/shard_map/reduce_scatter | solution.py:150
  370.5 0.0 copy-done.1
  (37 shorter events, 0.4 us)
Async XLA Ops:
  6.5 123.2 %copy-start = (bf16[4,128,128]{2,1,0:T(8,128)(2,1)S(1)}, bf16[4,128,128]{2,1,0:T(8,128)(2,1)}, u32[]{:S(2)}) copy-start(bf16[4,128,128]{2,1,0:T(8,128)(2,1)} %param.23) | copy-start | bytes 393220
  6.5 32.3 %all-gather.7.cloned.1.call-start = ((), (), s32[]{:S(2)}) async-start(), calls=%async_computation.1 | async-start | bytes 2359296 | tf_op jit(solution)/shard_map/all_gather | solution.py:53
  7.3 108.0 %all-gather.9.cloned.1.call-start = ((), (), s32[]{:S(2)}) async-start(), calls=%async_computation.2 | async-start | bytes 8912896 | tf_op jit(solution)/shard_map/all_gather | solution.py:48
  9.3 174.5 %all-gather.11.cloned.1.call-start = ((), (), s32[]{:S(2)}) async-start(), calls=%async_computation.3 | async-start | bytes 6684672 | tf_op jit(solution)/shard_map/all_gather | solution.py:75
  123.6 122.4 %all-gather.13.cloned.1.call-start = ((), (), s32[]{:S(2)}) async-start(), calls=%async_computation.4 | async-start | bytes 6684672 | tf_op jit(solution)/shard_map/all_gather | solution.py:76
  124.2 175.0 %all-gather.15.cloned.1.call-start = ((), (), s32[]{:S(2)}) async-start(), calls=%async_computation.5 | async-start | bytes 4456448 | tf_op jit(solution)/shard_map/all_gather | solution.py:49
  124.8 245.7 %reduce-scatter.2.cloned.1.call-start = ((), (), s32[]{:S(2)}) async-start(), calls=%async_computation.6 | async-start | bytes 2359296 | tf_op jit(solution)/shard_map/reduce_scatter | solution.py:150
  125.2 3.0 collective-permute-start
  128.5 1.3 copy-start.4
  252.7 11.9 %copy-start.2 = (f32[4]{0:T(128)S(1)}, f32[4]{0:T(128)}, u32[]{:S(2)}) copy-start(f32[4]{0:T(128)} %param.21) | copy-start | bytes 52
  264.0 0.8 copy-start.3
  299.3 71.2 %copy-start.1 = (bf16[4,128,128]{2,1,0:T(8,128)(2,1)S(1)}, bf16[4,128,128]{2,1,0:T(8,128)(2,1)}, u32[]{:S(2)}) copy-start(bf16[4,128,128]{2,1,0:T(8,128)(2,1)} %param.23) | copy-start | bytes 393220
Sparse Core Ops, SparseCore 0:
  8.9 29.8 all-gather.6
  41.0 74.2 all-gather.8
  123.8 59.9 all-gather.10
  185.9 60.0 all-gather.12
  248.0 51.1 all-gather.14
  304.6 65.8 reduce-scatter.1
where the time goes:
time: 378 us; the launch traced here: 377 us
  waiting for transfers between devices  306 us (81%)
  matrix products  22.3 us (6%)
  local copies, waits for them, and re-layouts  17.8 us (5%)
  between operations  13.7 us (4%)
  other arithmetic  8.77 us (2%)
  blocking collectives  5.5 us (1%)
    all_gather x1, waiting for transfers between devices, local(): lax.all_gather(w_cat, 'sp', axis=0, tiled=True)  74.7 us
    reduce_scatter x1, waiting for transfers between devices, local(): lax.psum_scatter(jnp.dot(branch, w_out_rows, preferred_element_type=jnp.f...  66 us
    all_gather x1, waiting for transfers between devices, local(): lax.all_gather(values, 'sp', axis=0, tiled=True)  53.6 us
    all_gather x1, waiting for transfers between devices, local(): lax.all_gather(key_rows, 'sp', axis=0, tiled=True)  52.3 us
    all_gather x1, waiting for transfers between devices, local(): lax.all_gather(w_out, 'sp', axis=1, tiled=True)  33.3 us
    all_gather x1, waiting for transfers between devices, local(): lax.all_gather(tokens, 'tp', axis=1, tiled=True)  24 us
    all_gather x1, local copies, waits for them, and re-layouts, local(): lax.all_gather(key_rows, 'sp', axis=0, tiled=True)  8.7 us
  transfers between devices with their start and end apart: 7, of which 7 were waited for; matrix products, arithmetic and copies ran while one was open for 9% of the time, Pallas kernels for 0%

commit v1 on v0

v1 whole, which is shorter than its diff:
```python
import functools
import math

import jax
import jax.numpy as jnp
from jax import lax
from jax.experimental import pallas as pl
from jax.experimental.pallas import tpu as pltpu
from jax.sharding import PartitionSpec as P

EPSILON = 1e-06
NEG_LARGE = -1e30
WINDOWS = (2, 4, 8, 16)
RIM_ROWS = 15


def passed_along(block, axis, distance):
    devices = range(lax.axis_size(axis))
    route = [(i - distance, i) for i in devices if i - distance in devices]
    return lax.ppermute(block, axis, route)


def attend(inner, vdim, hdim, member_ref, lam_ref, q_ref, kv_ref, gain_ref, out_ref, acc_ref, max_ref):
    rows = q_ref.shape[1]
    block = pl.program_id(0)
    last = block * inner + member_ref[0]
    scale = 1.0 / math.sqrt(hdim)
    queries = (q_ref[0].astype(jnp.float32) * scale).astype(jnp.bfloat16)
    maps = (queries[:, :hdim], queries[:, hdim:])
    ones = jnp.ones((rows, vdim), jnp.bfloat16)
    acc_ref[...] = jnp.zeros_like(acc_ref)
    max_ref[...] = jnp.full_like(max_ref, NEG_LARGE)

    def step(g, masked):
        keys_values = kv_ref[lax.rem(g, inner), lax.div(g, inner)]
        values = jnp.concatenate([keys_values[:, 2 * hdim :], ones], axis=1)
        for m in range(2):
            keys = keys_values[:, m * hdim : (m + 1) * hdim]
            scores = lax.dot_general(
                maps[m], keys, (((1,), (1,)), ((), ())), preferred_element_type=jnp.float32
            )
            if masked:
                row = lax.broadcasted_iota(jnp.int32, scores.shape, 0)
                col = lax.broadcasted_iota(jnp.int32, scores.shape, 1)
                scores = jnp.where(col <= row, scores, NEG_LARGE)
            old_max = max_ref[m]
            new_max = jnp.maximum(old_max, jnp.max(scores, axis=1, keepdims=True))
            factor = jnp.exp(old_max - new_max)
            expo = jnp.exp(scores - new_max[:, :1])
            acc_ref[m] = acc_ref[m] * factor[:, :1] + jnp.dot(
                expo.astype(jnp.bfloat16), values, preferred_element_type=jnp.float32
            )
            max_ref[m] = new_max

    def body(g, carry):
        step(g, False)
        return carry

    lax.fori_loop(0, last, body, 0)
    step(last, True)
    first = acc_ref[0]
    second = acc_ref[1]
    mix = first[:, :vdim] / first[:, vdim:] - lam_ref[0] * (second[:, :vdim] / second[:, vdim:])
    mean_sq = jnp.mean(mix * mix, axis=1, keepdims=True)
    out_ref[0] = (mix * lax.rsqrt(mean_sq + EPSILON) * gain_ref[...]).astype(jnp.bfloat16)


def flash(q, kv, member, lam, sub_gain):
    inner, outer, rows, width = kv.shape
    qdim = q.shape[-1]
    vdim = width - qdim
    smem = pl.BlockSpec(memory_space=pltpu.SMEM)
    work = outer * rows * outer * rows * inner
    return pl.pallas_call(
        functools.partial(attend, inner, vdim, qdim // 2),
        grid=(outer,),
        out_shape=jax.ShapeDtypeStruct((outer, rows, vdim), jnp.bfloat16),
        in_specs=[
            smem,
            smem,
            pl.BlockSpec((1, rows, qdim), lambda b: (b, 0, 0)),
            pl.BlockSpec(memory_space=pltpu.VMEM),
            pl.BlockSpec(memory_space=pltpu.VMEM),
        ],
        out_specs=pl.BlockSpec((1, rows, vdim), lambda b: (b, 0, 0)),
        scratch_shapes=[
            pltpu.VMEM((2, rows, 2 * vdim), jnp.float32),
            pltpu.VMEM((2, rows, 128), jnp.float32),
        ],
        compiler_params=pltpu.CompilerParams(vmem_limit_bytes=56 * 2**20),
        cost_estimate=pl.CostEstimate(
            flops=4 * work * vdim, bytes_accessed=kv.size * 2, transcendentals=work
        ),
    )(member, lam, q, kv, sub_gain.reshape(1, -1))


def trailing(x, window_ids, group_dim):
    column_window = jnp.repeat(window_ids, group_dim)[None, :]
    running = x
    picked = jnp.zeros_like(x)
    for slot, span in enumerate(WINDOWS):
        half = span // 2
        running = running + jnp.pad(running[:-half], ((half, 0), (0, 0)))
        picked = jnp.where(column_window == slot, running, picked)
    return picked


def local(
    tokens,
    pre_gain,
    w_query,
    w_key,
    w_value,
    w_pool,
    lambdas,
    sub_gain,
    group_weight,
    pool_scale,
    w_out,
):
    n_tp = lax.axis_size("tp")
    n_sp = lax.axis_size("sp")
    tp = lax.axis_index("tp")
    sp = lax.axis_index("sp")
    tok_rows = tokens.shape[0]
    model_width = tokens.shape[1] * n_tp
    heads = lambdas.shape[0]
    qdim = w_query.shape[1] // heads
    vdim = w_value.shape[1] // heads
    groups = group_weight.shape[0]
    group_dim = group_weight.shape[1]
    head_width = 2 * qdim + vdim
    outer = math.gcd(n_sp, heads)
    inner = n_sp // outer
    per_device = heads // outer

    pieces = []
    for h in range(heads):
        pieces += [
            w_query[:, h * qdim : (h + 1) * qdim],
            w_key[:, h * qdim : (h + 1) * qdim],
            w_value[:, h * vdim : (h + 1) * vdim],
        ]
    w_cat = jnp.concatenate(pieces + [w_pool], axis=1)
    w_in = lax.all_gather(w_cat, "sp", axis=0, tiled=True)
    w_out_rows = lax.all_gather(w_out, "sp", axis=1, tiled=True)

    features = tokens.astype(jnp.float32)
    mine = (features * pre_gain.astype(jnp.float32)[None, :]).astype(jnp.bfloat16)
    squares = jnp.sum(features * features, axis=1, keepdims=True)
    if n_tp == 2:
        swap = [(0, 1), (1, 0)]
        theirs = lax.ppermute(mine, "tp", swap)
        squares = squares + lax.ppermute(squares, "tp", swap)
        scaled = jnp.concatenate(
            [jnp.where(tp == 0, mine, theirs), jnp.where(tp == 0, theirs, mine)], axis=1
        )
    else:
        scaled = lax.all_gather(mine, "tp", axis=1, tiled=True)
        squares = lax.psum(squares, "tp")
    inverse = lax.rsqrt(squares / model_width + EPSILON)
    projected = (jnp.dot(scaled, w_in, preferred_element_type=jnp.float32) * inverse).astype(
        jnp.bfloat16
    )

    by_head = jnp.stack(
        [projected[:, h * head_width : (h + 1) * head_width] for h in range(heads)], axis=0
    )
    across = [[o * inner + i for o in range(outer)] for i in range(inner)]
    within = [[o * inner + i for i in range(inner)] for o in range(outer)]
    by_head = by_head.reshape(outer, per_device, tok_rows, head_width)
    if outer > 1:
        by_head = lax.all_to_all(by_head, "sp", 0, 0, axis_index_groups=across)
    kv = lax.all_gather(by_head[..., qdim:], "sp", axis=0, axis_index_groups=within)
    member = lax.rem(sp, inner).reshape(1)
    first_head = lax.div(sp, inner) * per_device
    attended = []
    for p in range(per_device):
        lam = lax.dynamic_slice_in_dim(lambdas, first_head + p, 1)
        attended.append(flash(by_head[:, p, :, :qdim], kv[:, :, p], member, lam, sub_gain))
    attended = jnp.stack(attended, axis=1)
    if outer > 1:
        attended = lax.all_to_all(attended, "sp", 0, 0, axis_index_groups=across)
    attended = attended.reshape(heads, tok_rows, vdim)

    pool_in = projected[:, heads * head_width :]
    halo = passed_along(pool_in[tok_rows - RIM_ROWS - 1 :], "sp", 1)
    extended = jnp.concatenate([halo, pool_in], axis=0).astype(jnp.float32)
    window_ids = (tp * groups + jnp.arange(groups, dtype=jnp.int32)) % len(WINDOWS)
    sums = trailing(extended, window_ids, group_dim)[RIM_ROWS + 1 :]
    spans = jnp.repeat(jnp.left_shift(2, window_ids), group_dim)
    positions = sp * tok_rows + jnp.arange(tok_rows, dtype=jnp.int32)
    count = jnp.minimum(positions[:, None] + 1, spans[None, :]).astype(jnp.float32)
    differ = (sums / count - pool_in.astype(jnp.float32)).astype(jnp.bfloat16)
    branch = []
    for g in range(groups):
        columns = slice(g * group_dim, (g + 1) * group_dim)
        pooled = jnp.dot(differ[:, columns], group_weight[g], preferred_element_type=jnp.float32)
        pooled = (pooled * pool_scale[columns][None, :]).astype(jnp.bfloat16)
        branch += [attended[g], pooled]
    branch = jnp.concatenate(branch, axis=1)
    partial = jnp.dot(branch, w_out_rows, preferred_element_type=jnp.float32)
    if n_tp == 2:
        half = tok_rows // 2
        keep = lax.dynamic_slice_in_dim(partial, tp * half, half, 0)
        send = lax.dynamic_slice_in_dim(partial, (1 - tp) * half, half, 0).astype(jnp.bfloat16)
        return (keep + lax.ppermute(send, "tp", swap).astype(jnp.float32)).astype(jnp.bfloat16)
    return lax.psum_scatter(partial.astype(jnp.bfloat16), "tp", scatter_dimension=0, tiled=True)


def solution(mesh):
    placed = (
        P("sp", "tp"),
        P("tp"),
        P("sp", "tp"),
        P("sp", "tp"),
        P("sp", "tp"),
        P("sp", "tp"),
        P("tp"),
        P(),
        P("tp", None, None),
        P("tp"),
        P("tp", "sp"),
    )
    return jax.shard_map(
        local, mesh=mesh, in_specs=placed, out_specs=P(("sp", "tp"), None), check_vma=False
    )
```

time: 378 us -> 261 us (0.69)
  waiting for transfers between devices: 306 us -> 127 us
  Pallas kernels: 0 us -> 36.1 us
  blocking collectives: 5.5 us -> 31.9 us
  starting transfers between devices: 2.35 us -> 10.6 us
  matrix products: 22.3 us -> 14.8 us
    all_gather x5 -> x3, waiting for transfers between devices: 238 us -> 77.4 us  [the longest x1 55.1 us: local(): w_in = lax.all_gather(w_cat, 'sp', axis=0, tiled=True)]
    reduce_scatter x1 -> x0, waiting for transfers between devices: 66 us -> none  [local(): lax.psum_scatter(jnp.dot(branch, w_out_rows, preferred_element_type=jnp.f...]
    pallas_call x0 -> x1, Pallas kernels: none -> 36.1 us  [flash(): pl.pallas_call(functools.partial(attend, inner, vdim, qdim // 2), grid=(o...]
    ppermute x0 -> x3, waiting for transfers between devices: none -> 34.9 us  [the longest x1 17.5 us: local(): squares = squares + lax.ppermute(squares, 'tp', swap)]
    all_to_all x0 -> x1, blocking collectives: none -> 31.9 us  [local(): by_head = lax.all_to_all(by_head, 'sp', 0, 0, axis_index_groups=across)]
    all_to_all x0 -> x1, waiting for transfers between devices: none -> 14.1 us  [local(): attended = lax.all_to_all(attended, 'sp', 0, 0, axis_index_groups=across)]
    all_gather x1 -> x0, local copies, waits for them, and re-layouts: 8.7 us -> none  [local(): lax.all_gather(key_rows, 'sp', axis=0, tiled=True)]
    dot_general x5 -> x6, matrix products: 22.3 us -> 14.8 us  [the longest x1 7.05 us: local(): jnp.dot(scaled, w_in, preferred_element_type=jnp.float32) * inverse]
  transfers between devices with their start and end apart: 7 -> 8, of which waited for: 7 -> 6; matrix products, arithmetic and copies ran while one was open for 9% -> 5% of each run, Pallas kernels for 0% -> 14%
where the time goes in v1:
time: 261 us; the launch traced here: 258 us
  waiting for transfers between devices  127 us (49%)
  Pallas kernels  36.1 us (14%)
  blocking collectives  31.9 us (12%)
  local copies, waits for them, and re-layouts  18.2 us (7%)
  matrix products  14.8 us (6%)
  between operations  13.3 us (5%)
  starting transfers between devices  10.6 us (4%)
  other arithmetic  5.7 us (2%)
    all_gather x1, waiting for transfers between devices, local(): w_in = lax.all_gather(w_cat, 'sp', axis=0, tiled=True)  55.1 us
    pallas_call x1, Pallas kernels, flash(): pl.pallas_call(functools.partial(attend, inner, vdim, qdim // 2), grid=(o...  36.1 us
    all_to_all x1, blocking collectives, local(): by_head = lax.all_to_all(by_head, 'sp', 0, 0, axis_index_groups=across)  31.9 us
    all_gather x1, waiting for transfers between devices, local(): lax.all_gather(by_head[..., qdim:], 'sp', axis=0, axis_index_groups=within)  22.3 us
    ppermute x1, waiting for transfers between devices, local(): squares = squares + lax.ppermute(squares, 'tp', swap)  17.5 us
    ppermute x1, waiting for transfers between devices, local(): lax.ppermute(send, 'tp', swap).astype(jnp.float32)  17.3 us
    all_to_all x1, waiting for transfers between devices, local(): attended = lax.all_to_all(attended, 'sp', 0, 0, axis_index_groups=across)  14.1 us
    unnamed x34, local copies, waits for them, and re-layouts  13.3 us
  transfers between devices with their start and end apart: 8, of which 6 were waited for; matrix products, arithmetic and copies ran while one was open for 5% of the time, Pallas kernels for 14%

profile of v1, /device:TPU:0, one launch (start us, length us, event | category | flops | bytes accessed | tf_op | source)
XLA Modules:
  0.0 257.8 jit_solution(14158978967013049345)
XLA Ops:
  6.5 0.8 constant_dynamic-update-slice_fusion.12
  7.4 0.8 constant_dynamic-update-slice_fusion.11
  8.2 0.8 constant_dynamic-update-slice_fusion.10
  8.9 0.8 constant_dynamic-update-slice_fusion.9
  9.7 0.8 constant_dynamic-update-slice_fusion.8
  10.5 0.8 constant_dynamic-update-slice_fusion.7
  11.2 0.8 constant_dynamic-update-slice_fusion.6
  12.0 0.8 constant_dynamic-update-slice_fusion.5
  12.8 0.8 constant_dynamic-update-slice_fusion.4
  13.6 0.8 constant_dynamic-update-slice_fusion.3
  14.3 0.8 constant_dynamic-update-slice_fusion.2
  15.1 0.8 constant_dynamic-update-slice_fusion.1
  15.9 0.9 constant_dynamic-update-slice_fusion
  16.8 0.8 copy-done.2
  17.7 0.0 all-gather.9.cloned.1.call-start
  17.8 0.3 fusion.1
  18.1 3.0 %collective-permute-start = (bf16[384,1024]{1,0:T(8,128)(2,1)S(1)}, bf16[384,1024]{1,0:T(8,128)(2,1)S(1)}, u32[]{:S(2)}, u32[]{:S(2)}) collective-permute-start(bf16[384,1024]{1,0:T(8,128)(2,1)S(1)} %get-tuple-element.12), channel_id=1, source_target_pairs={{0,1},{1,0},{2,3},{3,2},{4,5},{5,4},{6,7},{7,6},{8,9},{9,8},{10,11... | collective-permute-start | bytes 2359304 | tf_op jit(solution)/shard_map/ppermute | solution.py:153
  21.1 0.1 collective-permute-start.1
  21.2 17.5 %collective-permute-done.1 = f32[384,1]{0,1:T(1,128)S(1)} collective-permute-done((f32[384,1]{0,1:T(1,128)S(1)}, f32[384,1]{0,1:T(1,128)S(1)}, u32[]{:S(2)}, u32[]{:S(2)}) %collective-permute-start.1) | collective-permute-done | bytes 1568 | tf_op jit(solution)/shard_map/ppermute | solution.py:154
  38.7 1.0 broadcast_select_fusion.1
  39.7 55.1 %all-gather.5.cloned.1.call-done = bf16[2048,2048]{1,0:T(8,128)(2,1)} async-done(((bf16[128,2048]{1,0:T(8,128)(2,1)}), bf16[2048,2048]{1,0:T(8,128)(2,1)}) %all-gather.5.cloned.1.call-update) | async-done | bytes 8388624 | tf_op jit(solution)/shard_map/all_gather | solution.py:145
  94.8 7.0 %multiply_convert_fusion = bf16[384,2048]{1,0:T(8,128)(2,1)S(1)} fusion(bf16[2048,2048]{1,0:T(8,128)(2,1)} %all-gather.5.cloned.1.call-done, bf16[384,1024]{1,0:T(8,128)(2,1)} %get-tuple-element.10, bf16[384,1024]{1,0:T(8,128)(2,1)S(1)} %get-tuple-element.9, f32[384]{0:T(512)S(1)} %rsqrt_reduce_fusion), kind=kOutput, calls=%fused_computation | convolution fusion | flops 3225944064 | bytes 11535872 | tf_op jit(solution)/shard_map/dot_general | solution.py:162
  101.9 0.1 slice_bitcast_fusion.4
  102.0 0.2 maximum_bitcast_fusion
  102.2 31.9 %all_to_all.10 = bf16[4,1,384,384]{3,2,1,0:T(8,128)(2,1)S(1)} all-to-all(bf16[4,1,384,384]{3,2,1,0:T(8,128)(2,1)S(1)} %maximum_bitcast_fusion), channel_id=1, replica_groups={{0,8,16,24},{2,10,18,26},{4,12,20,28},{6,14,22,30},{1,9,17,25},{3,11,19..., dimensions={0} | all-to-all | bytes 2359296 | tf_op jit(solution)/shard_map/all_to_all | solution.py:173
  134.2 0.9 slice.174
  135.1 0.0 all-gather.7.cloned.1.call-start
  135.2 0.7 all-gather.7.cloned.1.call-update
  135.9 0.1 broadcast_bitcast_fusion.1
  136.0 0.1 broadcast_bitcast_fusion.2
  136.1 0.1 broadcast_bitcast_fusion.3
  136.1 0.1 broadcast_bitcast_fusion.4
  136.2 0.1 broadcast_bitcast_fusion
  136.3 1.3 collective-permute-start.2
  137.6 0.6 dynamic_slice.9.lam_ref
  138.3 0.1 collective-permute-done.2
  138.4 0.1 maximum_convert_fusion
  138.5 0.1 pad_add_fusion.2
  138.7 0.2 pad_add_fusion.1
  138.8 0.8 slice_bitcast_fusion.q_ref
  139.7 22.3 %all-gather.9.cloned.1.call-done = bf16[16,1,384,256]{3,2,1,0:T(8,128)(2,1)} async-done(((bf16[4,1,384,256]{3,2,1,0:T(8,128)(2,1)}), bf16[16,1,384,256]{3,2,1,0:T(8,128)(2,1)}) %all-gather.9.cloned.1.call-update) | async-done | bytes 3145744 | tf_op jit(solution)/shard_map/all_gather | solution.py:174
  162.0 36.1 %shard_map.109 = bf16[4,384,128]{2,1,0:T(8,128)(2,1)} custom-call(s32[1]{0:T(128)} %bitcast.member_ref, f32[1]{0:T(128)} %dynamic_slice.9.lam_ref, bf16[4,384,128]{2,1,0:T(8,128)(2,1)} %slice_bitcast_fusion.q_ref, bf16[4,4,384,256]{3,2,1,0:T(8,128)(2,1)} %bitcast.62, f32[1,128]{1,0:T(1,128)} %bitcast.63), custom_call_target="tpu_custom_call" | custom-call | flops 4831838208 | bytes 3145728 | tf_op jit(solution)/shard_map/pallas_call | solution.py:74
  198.1 4.6 %all-to-all-start.1 = ((bf16[4,1,384,128]{3,2,1,0:T(8,128)(2,1)}), bf16[4,1,384,128]{3,2,1,0:T(8,128)(2,1)S(1)}, u32[]{:S(2)}, u32[]{:S(2)}) async-start(bf16[4,1,384,128]{3,2,1,0:T(8,128)(2,1)} %bitcast.61), calls=%async_computation.1 | async-start | bytes 786432 | tf_op jit(solution)/shard_map/all_to_all | solution.py:183
  202.7 0.2 pad_add_fusion
  202.8 0.1 slice.181
  202.9 1.4 fusion.17
  204.3 14.1 %all-to-all-done.1 = bf16[4,1,384,128]{3,2,1,0:T(8,128)(2,1)S(1)} async-done(((bf16[4,1,384,128]{3,2,1,0:T(8,128)(2,1)}), bf16[4,1,384,128]{3,2,1,0:T(8,128)(2,1)S(1)}, u32[]{:S(2)}, u32[]{:S(2)}) %all-to-all-start.1) | async-done | bytes 393248 | tf_op jit(solution)/shard_map/all_to_all | solution.py:183
  218.4 0.1 copy.25
  218.5 0.1 copy.26
  218.7 0.1 copy.27
  218.8 0.1 copy.28
  218.9 0.7 bitcast_dynamic-update-slice_fusion.3
  219.6 0.9 fusion.6
  220.5 0.7 bitcast_dynamic-update-slice_fusion.2
  221.1 0.9 fusion.8
  222.0 0.7 bitcast_dynamic-update-slice_fusion.1
  222.6 0.9 fusion.10
  223.5 0.7 bitcast_dynamic-update-slice_fusion
  224.1 0.9 fusion.12
  225.0 4.3 %fusion.34 = f32[384,2048]{1,0:T(8,128)S(1)} fusion(bf16[384,1024]{0,1:T(8,128)(2,1)} %fusion.12, bf16[1024,2048]{1,0:T(8,128)(2,1)} %all-gather.7.cloned.1.call-done), kind=kOutput, calls=%fused_computation.90 | convolution fusion | flops 1610612736 | bytes 8126464 | tf_op jit(solution)/shard_map/dot_general | solution.py:202
  229.3 1.0 dynamic-slice_convert_fusion
  230.3 1.5 collective-permute-start.3
  231.8 17.3 %collective-permute-done.3 = bf16[192,2048]{1,0:T(8,128)(2,1)} collective-permute-done((bf16[192,2048]{1,0:T(8,128)(2,1)}, bf16[192,2048]{1,0:T(8,128)(2,1)}, u32[]{:S(2)}, u32[]{:S(2)}) %collective-permute-start.3) | collective-permute-done | bytes 786464 | tf_op jit(solution)/shard_map/ppermute | solution.py:207
  249.1 2.2 add_convert_fusion
  (29 shorter events, 0.2 us)
Async XLA Ops:
  6.5 11.2 %copy-start.3 = (bf16[1024]{0:T(1024)(128)(2,1)S(1)}, bf16[1024]{0:T(1024)(128)(2,1)}, u32[]{:S(2)}) copy-start(bf16[1024]{0:T(1024)(128)(2,1)} %param.12) | copy-start | bytes 6148
  6.5 11.2 %copy-start.1 = (bf16[384,1024]{1,0:T(8,128)(2,1)S(1)}, bf16[384,1024]{1,0:T(8,128)(2,1)}, u32[]{:S(2)}) copy-start(bf16[384,1024]{1,0:T(8,128)(2,1)} %param.11) | copy-start | bytes 2359300
  6.5 88.3 %all-gather.5.cloned.1.call-start = ((), (), s32[]{:S(2)}) async-start(), calls=%async_computation.2 | async-start | bytes 8912896 | tf_op jit(solution)/shard_map/all_gather | solution.py:145
  16.8 0.9 copy-start.2
  17.7 144.3 %all-gather.9.cloned.1.call-start = ((), (), s32[]{:S(2)}) async-start(), calls=%async_computation.4 | async-start | bytes 3932160 | tf_op jit(solution)/shard_map/all_gather | solution.py:174
  18.1 20.7 %collective-permute-start = (bf16[384,1024]{1,0:T(8,128)(2,1)S(1)}, bf16[384,1024]{1,0:T(8,128)(2,1)S(1)}, u32[]{:S(2)}, u32[]{:S(2)}) collective-permute-start(bf16[384,1024]{1,0:T(8,128)(2,1)S(1)} %get-tuple-element.12), channel_id=1, source_target_pairs={{0,1},{1,0},{2,3},{3,2},{4,5},{5,4},{6,7},{7,6},{8,9},{9,8},{10,11... | collective-permute-start | bytes 2359304 | tf_op jit(solution)/shard_map/ppermute | solution.py:153
  21.1 17.6 %collective-permute-start.1 = (f32[384,1]{0,1:T(1,128)S(1)}, f32[384,1]{0,1:T(1,128)S(1)}, u32[]{:S(2)}, u32[]{:S(2)}) collective-permute-start(f32[384,1]{0,1:T(1,128)S(1)} %broadcast_in_dim.47), channel_id=1, source_target_pairs={{0,1},{1,0},{2,3},{3,2},{4,5},{5,4},{6,7},{7,6},{8,9},{9,8},{10,11... | collective-permute-start | bytes 4616 | tf_op jit(solution)/shard_map/ppermute | solution.py:154
  101.9 36.4 %copy-start = (bf16[384,2048]{1,0:T(8,128)(2,1)}, bf16[384,2048]{1,0:T(8,128)(2,1)S(1)}, u32[]{:S(2)}) copy-start(bf16[384,2048]{1,0:T(8,128)(2,1)S(1)} %multiply_convert_fusion) | copy-start | bytes 4718596
  134.2 2.1 copy-start.4
  134.2 3.5 %copy-start.6 = (f32[4]{0:T(128)S(1)}, f32[4]{0:T(128)}, u32[]{:S(2)}) copy-start(f32[4]{0:T(128)} %param.17) | copy-start | bytes 52
  135.1 89.9 %all-gather.7.cloned.1.call-start = ((), (), s32[]{:S(2)}) async-start(), calls=%async_computation.3 | async-start | bytes 4456448 | tf_op jit(solution)/shard_map/all_gather | solution.py:146
  136.3 2.1 collective-permute-start.2
  198.1 20.3 %all-to-all-start.1 = ((bf16[4,1,384,128]{3,2,1,0:T(8,128)(2,1)}), bf16[4,1,384,128]{3,2,1,0:T(8,128)(2,1)S(1)}, u32[]{:S(2)}, u32[]{:S(2)}) async-start(bf16[4,1,384,128]{3,2,1,0:T(8,128)(2,1)} %bitcast.61), calls=%async_computation.1 | async-start | bytes 786432 | tf_op jit(solution)/shard_map/all_to_all | solution.py:183
  204.3 15.3 %copy-start.5 = (bf16[4,128,128]{2,1,0:T(8,128)(2,1)S(1)}, bf16[4,128,128]{2,1,0:T(8,128)(2,1)}, u32[]{:S(2)}) copy-start(bf16[4,128,128]{2,1,0:T(8,128)(2,1)} %param.19) | copy-start | bytes 393220
  230.3 18.9 %collective-permute-start.3 = (bf16[192,2048]{1,0:T(8,128)(2,1)}, bf16[192,2048]{1,0:T(8,128)(2,1)}, u32[]{:S(2)}, u32[]{:S(2)}) collective-permute-start(bf16[192,2048]{1,0:T(8,128)(2,1)} %dynamic-slice_convert_fusion), channel_id=1, source_target_pairs={{0,1},{1,0},{2,3},{3,2},{4,5},{5,4},{6,7},{7,6},{8,9},{9,8},{10,11... | collective-permute-start | bytes 2359304 | tf_op jit(solution)/shard_map/ppermute | solution.py:207
Sparse Core Ops, SparseCore 0:
  17.8 77.0 all-gather.4
  135.2 26.6 all-gather.8
  164.1 58.8 all-gather.6

commit v2 on v1

--- a/solution.py
+++ b/solution.py
@@ -92,6 +92,205 @@
             flops=4 * work * vdim, bytes_accessed=kv.size * 2, transcendentals=work
         ),
     )(member, lam, q, kv, sub_gain.reshape(1, -1))
+
+
+def spread(n_sp, count, with_swap, *refs):
+    weights, refs = refs[:count], refs[count:]
+    mine, refs = refs[0], refs[1:]
+    fulls, refs = refs[:count], refs[count:]
+    theirs, refs = refs[0], refs[1:]
+    up_send, up_recv, down_send, down_recv, y_send, y_recv, c_send, c_recv, own_sem, swap_sem = refs
+    depth = n_sp // 4
+    rows = weights[0].shape[0]
+    sp = lax.axis_index("sp")
+    z = lax.div(sp, 4)
+    y = lax.rem(lax.div(sp, 2), 2)
+    c = lax.rem(sp, 2)
+    y_peer = z * 4 + (1 - y) * 2 + c
+    c_peer = z * 4 + y * 2 + (1 - c)
+    barrier = pltpu.get_barrier_semaphore()
+
+    def greet(device):
+        pl.semaphore_signal(barrier, 1, device_id=device, device_id_type=pl.DeviceIdType.MESH)
+
+    greet({"sp": y_peer})
+    greet({"sp": c_peer})
+    greeted = 2
+    if with_swap:
+        greet({"tp": 1 - lax.axis_index("tp")})
+        greeted = 3
+
+    @pl.when(z > 0)
+    def _():
+        greet({"sp": sp - 4})
+
+    @pl.when(z < depth - 1)
+    def _():
+        greet({"sp": sp + 4})
+
+    in_line = jnp.where(z > 0, 1, 0) + jnp.where(z < depth - 1, 1, 0)
+    pl.semaphore_wait(barrier, greeted + in_line)
+
+    def slot(a, zz, yy, cc):
+        start = pl.multiple_of((zz * 4 + yy * 2 + cc) * rows, rows)
+        return fulls[a].at[pl.ds(start, rows), :]
+
+    def remote(src, dst, send, recv, device):
+        return pltpu.make_async_remote_copy(
+            src_ref=src,
+            dst_ref=dst,
+            send_sem=send,
+            recv_sem=recv,
+            device_id=device,
+            device_id_type=pl.DeviceIdType.MESH,
+        )
+
+    def line_copy(side, k, a, src):
+        sends, recvs = (up_send, up_recv) if side > 0 else (down_send, down_recv)
+        there = slot(a, z - side * k, y, c)
+        return remote(
+            there if src is None else src,
+            there,
+            sends.at[k, a],
+            recvs.at[k + 1, a],
+            {"sp": sp + 4 * side},
+        )
+
+    def y_copy(zz, yy, a, src):
+        there = slot(a, zz, yy, c)
+        src = there if src is None else src
+        return remote(src, there, y_send.at[zz, a], y_recv.at[zz, a], {"sp": y_peer})
+
+    def c_copy(zz, yy, cc, a, src):
+        there = slot(a, zz, yy, cc)
+        src = there if src is None else src
+        return remote(src, there, c_send.at[zz, yy, a], c_recv.at[zz, yy, a], {"sp": c_peer})
+
+    def can_go(side):
+        return z < depth - 1 if side > 0 else z > 0
+
+    def came(side, k):
+        return z >= k if side > 0 else z + k <= depth - 1
+
+    if with_swap:
+        swap = remote(
+            mine, theirs, swap_sem.at[0], swap_sem.at[1], {"tp": 1 - lax.axis_index("tp")}
+        )
+        swap.start()
+    for a in range(count):
+        for side in (1, -1):
+
+            @pl.when(can_go(side))
+            def _():
+                line_copy(side, 0, a, weights[a]).start()
+
+        y_copy(z, y, a, weights[a]).start()
+    for a in range(count):
+        c_copy(z, y, c, a, weights[a]).start()
+        pltpu.make_async_copy(weights[a], slot(a, z, y, c), own_sem.at[a]).start()
+
+    def from_pair(zz):
+        for a in range(count):
+            y_copy(zz, 1 - y, a, None).wait_recv()
+            c_copy(zz, 1 - y, c, a, None).start()
+
+    def relay(k, carry):
+        for side in (1, -1):
+            recvs = up_recv if side > 0 else down_recv
+
+            @pl.when(came(side, k))
+            def _():
+                zz = z - side * k
+                for a in range(count):
+                    there = slot(a, zz, y, c)
+                    remote(there, there, up_send.at[0, a], recvs.at[k, a], {"sp": y_peer}).wait_recv()
+
+                    @pl.when(can_go(side))
+                    def _():
+                        line_copy(side, k, a, None).start()
+
+                    y_copy(zz, y, a, None).start()
+                    c_copy(zz, y, c, a, None).start()
+
+        @pl.when(k == 1)
+        def _():
+            from_pair(z)
+
+        for side in (1, -1):
+
+            @pl.when((k > 1) & came(side, k - 1))
+            def _():
+                from_pair(z - side * (k - 1))
+
+        return carry
+
+    lax.fori_loop(1, depth, relay, 0)
+    if depth == 1:
+        from_pair(z)
+    for side in (1, -1):
+        if depth > 1:
+
+            @pl.when(came(side, depth - 1))
+            def _():
+                from_pair(z - side * (depth - 1))
+
+    def drain(zz, carry):
+        for a in range(count):
+            y_copy(zz, y, a, None).wait_send()
+            for yy in range(2):
+                c_copy(zz, yy, 1 - c, a, None).wait_recv()
+                c_copy(zz, yy, c, a, None).wait_send()
+        return carry
+
+    lax.fori_loop(0, depth, drain, 0)
+
+    def drain_line(k, carry):
+        for side in (1, -1):
+
+            @pl.when(came(side, k) & can_go(side))
+            def _():
+                for a in range(count):
+                    line_copy(side, k, a, None).wait_send()
+
+        return carry
+
+    lax.fori_loop(0, depth, drain_line, 0)
+    for a in range(count):
+        pltpu.make_async_copy(weights[a], slot(a, z, y, c), own_sem.at[a]).wait()
+    if with_swap:
+        swap.wait()
+
+
+def gather_weights(weights, mine, with_swap):
+    n_sp = lax.axis_size("sp")
+    count = len(weights)
+    depth = n_sp // 4
+    sems = pltpu.SemaphoreType.DMA
+    any_spec = pl.BlockSpec(memory_space=pl.ANY)
+    vmem_spec = pl.BlockSpec(memory_space=pltpu.VMEM)
+    shapes = [jax.ShapeDtypeStruct((n_sp * w.shape[0], w.shape[1]), w.dtype) for w in weights]
+    shapes.append(jax.ShapeDtypeStruct(mine.shape, mine.dtype))
+    moved = sum(w.size for w in weights) * 2 * n_sp
+    return pl.pallas_call(
+        functools.partial(spread, n_sp, count, with_swap),
+        out_shape=shapes,
+        in_specs=[vmem_spec] * (count + 1),
+        out_specs=[any_spec] * (count + 1),
+        scratch_shapes=[
+            sems((depth + 1, count)),
+            sems((depth + 1, count)),
+            sems((depth + 1, count)),
+            sems((depth + 1, count)),
+            sems((depth, count)),
+            sems((depth, count)),
+            sems((depth, 2, count)),
+            sems((depth, 2, count)),
+            sems((count,)),
+            sems((2,)),
+        ],
+        compiler_params=pltpu.CompilerParams(collective_id=0, has_side_effects=True),
+        cost_estimate=pl.CostEstimate(flops=10**10, bytes_accessed=moved, transcendentals=0),
+    )(*weights, mine)
 
 
 def trailing(x, window_ids, group_dim):
@@ -134,23 +333,20 @@
     inner = n_sp // outer
     per_device = heads // outer
 
-    pieces = []
-    for h in range(heads):
-        pieces += [
-            w_query[:, h * qdim : (h + 1) * qdim],
-            w_key[:, h * qdim : (h + 1) * qdim],
-            w_value[:, h * vdim : (h + 1) * vdim],
-        ]
-    w_cat = jnp.concatenate(pieces + [w_pool], axis=1)
-    w_in = lax.all_gather(w_cat, "sp", axis=0, tiled=True)
-    w_out_rows = lax.all_gather(w_out, "sp", axis=1, tiled=True)
-
     features = tokens.astype(jnp.float32)
     mine = (features * pre_gain.astype(jnp.float32)[None, :]).astype(jnp.bfloat16)
     squares = jnp.sum(features * features, axis=1, keepdims=True)
+    swap = [(0, 1), (1, 0)]
+    weights = [w_query, w_key, w_value, w_pool]
+    if n_sp % 4 == 0:
+        *weights, theirs = gather_weights(weights, mine, n_tp == 2)
+    else:
+        weights = [lax.all_gather(w, "sp", axis=0, tiled=True) for w in weights]
+        theirs = lax.ppermute(mine, "tp", swap) if n_tp == 2 else mine
+    w_sorted = w_out.reshape(heads, 2, vdim, -1).swapaxes(0, 1).reshape(w_out.shape)
+    w_sorted, weights = lax.optimization_barrier((w_sorted, weights))
+    w_out_rows = lax.all_gather(w_sorted, "sp", axis=1, tiled=True)
     if n_tp == 2:
-        swap = [(0, 1), (1, 0)]
-        theirs = lax.ppermute(mine, "tp", swap)
         squares = squares + lax.ppermute(squares, "tp", swap)
         scaled = jnp.concatenate(
             [jnp.where(tp == 0, mine, theirs), jnp.where(tp == 0, theirs, mine)], axis=1
@@ -159,12 +355,16 @@
         scaled = lax.all_gather(mine, "tp", axis=1, tiled=True)
         squares = lax.psum(squares, "tp")
     inverse = lax.rsqrt(squares / model_width + EPSILON)
-    projected = (jnp.dot(scaled, w_in, preferred_element_type=jnp.float32) * inverse).astype(
-        jnp.bfloat16
-    )
-
-    by_head = jnp.stack(
-        [projected[:, h * head_width : (h + 1) * head_width] for h in range(heads)], axis=0
+    queries, key_rows, values, pool_in = [
+        (jnp.dot(scaled, w, preferred_element_type=jnp.float32) * inverse).astype(jnp.bfloat16)
+        for w in weights
+    ]
+    by_head = jnp.concatenate(
+        [
+            x.reshape(tok_rows, heads, -1).swapaxes(0, 1)
+            for x in (queries, key_rows, values)
+        ],
+        axis=2,
     )
     across = [[o * inner + i for o in range(outer)] for i in range(inner)]
     within = [[o * inner + i for i in range(inner)] for o in range(outer)]
@@ -183,7 +383,6 @@
         attended = lax.all_to_all(attended, "sp", 0, 0, axis_index_groups=across)
     attended = attended.reshape(heads, tok_rows, vdim)
 
-    pool_in = projected[:, heads * head_width :]
     halo = passed_along(pool_in[tok_rows - RIM_ROWS - 1 :], "sp", 1)
     extended = jnp.concatenate([halo, pool_in], axis=0).astype(jnp.float32)
     window_ids = (tp * groups + jnp.arange(groups, dtype=jnp.int32)) % len(WINDOWS)
@@ -192,13 +391,16 @@
     positions = sp * tok_rows + jnp.arange(tok_rows, dtype=jnp.int32)
     count = jnp.minimum(positions[:, None] + 1, spans[None, :]).astype(jnp.float32)
     differ = (sums / count - pool_in.astype(jnp.float32)).astype(jnp.bfloat16)
-    branch = []
-    for g in range(groups):
-        columns = slice(g * group_dim, (g + 1) * group_dim)
-        pooled = jnp.dot(differ[:, columns], group_weight[g], preferred_element_type=jnp.float32)
-        pooled = (pooled * pool_scale[columns][None, :]).astype(jnp.bfloat16)
-        branch += [attended[g], pooled]
-    branch = jnp.concatenate(branch, axis=1)
+    pooled = jnp.einsum(
+        "tgc,gcd->tgd",
+        differ.reshape(tok_rows, groups, group_dim),
+        group_weight,
+        preferred_element_type=jnp.float32,
+    )
+    pooled = (pooled * pool_scale.reshape(groups, group_dim)).astype(jnp.bfloat16)
+    branch = jnp.concatenate(
+        [attended.swapaxes(0, 1).reshape(tok_rows, -1), pooled.reshape(tok_rows, -1)], axis=1
+    )
     partial = jnp.dot(branch, w_out_rows, preferred_element_type=jnp.float32)
     if n_tp == 2:
         half = tok_rows // 2

time: 261 us -> 233 us (0.89); the launches traced: 258 us -> 233 us
  waiting for transfers between devices: 127 us -> 55.7 us
  Pallas kernels: 36.1 us -> 88.8 us
  local copies, waits for them, and re-layouts: 18.2 us -> 7.43 us
    pallas_call x0 -> x1, Pallas kernels: none -> 52.7 us  [gather_weights(): pl.pallas_call(functools.partial(spread, n_sp, count, with_swap), out_sha...]
    all_gather x2 -> x1, waiting for transfers between devices: 55.1 us -> 3.44 us  [local(): w_out_rows = lax.all_gather(w_sorted, 'sp', axis=1, tiled=True)]
    ppermute x1, waiting for transfers between devices: 17.5 us -> 0.01 us  [local(): squares = squares + lax.ppermute(squares, 'tp', swap)]
    unnamed x34 -> x14, local copies, waits for them, and re-layouts: 13.3 us -> 0.46 us
    all_gather x1, waiting for transfers between devices: 22.3 us -> 19 us  [local(): lax.all_gather(by_head[..., qdim:], 'sp', axis=0, axis_index_groups=within)]
    ppermute x1 -> x0, starting transfers between devices: 3.02 us -> none  [local(): theirs = lax.ppermute(mine, 'tp', swap)]
    ppermute x1, starting transfers between devices: 0.09 us -> 2.97 us  [local(): squares = squares + lax.ppermute(squares, 'tp', swap)]
  transfers between devices with their start and end apart: 8 -> 6, of which waited for: 6 -> 5; matrix products, arithmetic and copies ran while one was open for 5% -> 4% of each run, Pallas kernels for 14% -> 38%
where the time goes in v2:
time: 233 us
  Pallas kernels  88.8 us (38%)
  waiting for transfers between devices  55.7 us (24%)
  blocking collectives  33.5 us (14%)
  matrix products  16.2 us (7%)
  between operations  13.7 us (6%)
  starting transfers between devices  10.3 us (4%)
  local copies, waits for them, and re-layouts  7.43 us (3%)
  other arithmetic  7.18 us (3%)
    pallas_call x1, Pallas kernels, gather_weights(): pl.pallas_call(functools.partial(spread, n_sp, count, with_swap), out_sha...  52.7 us
    pallas_call x1, Pallas kernels, flash(): pl.pallas_call(functools.partial(attend, inner, vdim, qdim // 2), grid=(o...  36.1 us
    all_to_all x1, blocking collectives, local(): by_head = lax.all_to_all(by_head, 'sp', 0, 0, axis_index_groups=across)  33.5 us
    all_gather x1, waiting for transfers between devices, local(): lax.all_gather(by_head[..., qdim:], 'sp', axis=0, axis_index_groups=within)  19 us
    ppermute x1, waiting for transfers between devices, local(): lax.ppermute(send, 'tp', swap).astype(jnp.float32)  18.7 us
    all_to_all x1, waiting for transfers between devices, local(): attended = lax.all_to_all(attended, 'sp', 0, 0, axis_index_groups=across)  13.7 us
    dot_general x4, matrix products, local(): jnp.dot(scaled, w, preferred_element_type=jnp.float32) * inverse  10.5 us
    all_to_all x1, starting transfers between devices, local(): attended = lax.all_to_all(attended, 'sp', 0, 0, axis_index_groups=across)  4.71 us
  transfers between devices with their start and end apart: 6, of which 5 were waited for; matrix products, arithmetic and copies ran while one was open for 4% of the time, Pallas kernels for 38%

profile of v2, /device:TPU:0, one launch (start us, length us, event | category | flops | bytes accessed | tf_op | source)
XLA Modules:
  0.0 232.9 jit_solution(16468105509278288781)
XLA Ops:
  6.5 0.0 copy-start
  6.5 0.0 all-gather.6.cloned.1.call-start
  6.5 0.7 convert_element_type.57
  7.3 2.2 fusion.1
  9.5 3.0 %collective-permute-start = (f32[384,1]{0,1:T(1,128)S(1)}, f32[384,1]{0,1:T(1,128)S(1)}, u32[]{:S(2)}, u32[]{:S(2)}) collective-permute-start(f32[384,1]{0,1:T(1,128)S(1)} %broadcast_in_dim.43), channel_id=1, source_target_pairs={{0,1},{1,0},{2,3},{3,2},{4,5},{5,4},{6,7},{7,6},{8,9},{9,8},{10,11... | collective-permute-start | bytes 4616 | tf_op jit(solution)/shard_map/ppermute | solution.py:350
  12.5 0.0 copy-start.1
  12.5 52.7 %shard_map.109 = (bf16[2048,512]{1,0:T(8,128)(2,1)}, bf16[2048,512]{1,0:T(8,128)(2,1)}, bf16[2048,512]{1,0:T(8,128)(2,1)}, bf16[2048,512]{1,0:T(8,128)(2,1)}, bf16[384,1024]{1,0:T(8,128)(2,1)}) custom-call(bf16[128,512]{1,0:T(8,128)(2,1)} %refs_0_.1, bf16[128,512]{1,0:T(8,128)(2,1)} %refs_1_.1, bf16[128,512]{1,0:T(8,128)(2,1)} %refs_2_.1, ...), custom_call_target="tpu_custom_call" | custom-call | flops 10000000000 | bytes 8388608 | tf_op jit(solution)/shard_map/pallas_call | solution.py:274
  65.2 0.0 copy-start.4
  65.2 0.0 copy-done.1
  65.2 1.3 broadcast_select_fusion.1
  66.5 0.0 copy-start.2
  66.5 0.0 copy-done.4
  66.5 0.8 copy.33
  67.3 0.0 collective-permute-done
  67.3 2.6 %fusion.2 = bf16[384,512]{1,0:T(8,128)(2,1)S(1)} fusion(bf16[2048,512]{1,0:T(8,128)(2,1)} %get-tuple-element.20, f32[384]{0:T(512)S(1)} %rsqrt_reduce_fusion, bf16[384,1024]{1,0:T(8,128)(2,1)S(1)} %get-tuple-element.26, bf16[384,1024]{1,0:T(8,128)(2,1)S(1)} %get-tuple-element.25), kind=kOutput, calls=%fused_computation.12 | convolution fusion | flops 808845312 | bytes 4064768 | tf_op jit(solution)/shard_map/dot_general | solution.py:359
  69.9 0.2 copy.34
  70.1 0.0 copy-done.2
  70.1 2.6 %fusion.3 = bf16[384,512]{1,0:T(8,128)(2,1)S(1)} fusion(bf16[2048,512]{1,0:T(8,128)(2,1)} %get-tuple-element.21, f32[384]{0:T(512)S(1)} %rsqrt_reduce_fusion, bf16[384,1024]{1,0:T(8,128)(2,1)S(1)} %get-tuple-element.26, bf16[384,1024]{1,0:T(8,128)(2,1)S(1)} %get-tuple-element.25), kind=kOutput, calls=%fused_computation.13 | convolution fusion | flops 808845312 | bytes 4064768 | tf_op jit(solution)/shard_map/dot_general | solution.py:359
  72.7 0.2 copy.35
  72.9 2.8 %fusion.4 = bf16[384,512]{1,0:T(8,128)(2,1)S(1)} fusion(bf16[2048,512]{1,0:T(8,128)(2,1)} %get-tuple-element.22, f32[384]{0:T(512)S(1)} %rsqrt_reduce_fusion, bf16[384,1024]{1,0:T(8,128)(2,1)} %copy-done.2, bf16[384,1024]{1,0:T(8,128)(2,1)S(1)} %get-tuple-element.25), kind=kOutput, calls=%fused_computation.14 | convolution fusion | flops 808845312 | bytes 4064768 | tf_op jit(solution)/shard_map/dot_general | solution.py:359
  75.7 0.2 copy.36
  76.0 0.1 maximum_bitcast_fusion
  76.1 0.8 copy.37
  76.9 33.5 %all_to_all.10 = bf16[4,1,384,384]{3,2,1,0:T(8,128)(2,1)S(1)} all-to-all(bf16[4,1,384,384]{3,2,1,0:T(8,128)(2,1)S(1)} %copy.37), channel_id=1, replica_groups={{0,8,16,24},{2,10,18,26},{4,12,20,28},{6,14,22,30},{1,9,17,25},{3,11,19..., dimensions={0} | all-to-all | bytes 2359296 | tf_op jit(solution)/shard_map/all_to_all | solution.py:373
  110.4 0.0 copy-start.3
  110.4 0.9 slice.33
  111.4 0.0 all-gather.6.cloned.1.call-update
  111.4 0.0 all-gather.4.cloned.1.call-start
  111.4 0.7 all-gather.4.cloned.1.call-update
  112.2 0.1 broadcast_bitcast_fusion.1
  112.3 0.1 broadcast_bitcast_fusion.2
  112.4 0.1 broadcast_bitcast_fusion.3
  112.4 0.1 broadcast_bitcast_fusion.4
  112.5 0.1 broadcast_bitcast_fusion
  112.6 0.0 copy-done.3
  112.6 0.0 copy-start.6
  112.6 2.6 %fusion.5 = bf16[384,512]{1,0:T(8,128)(2,1)S(1)} fusion(bf16[2048,512]{1,0:T(8,128)(2,1)} %get-tuple-element.23, f32[384]{0:T(512)S(1)} %rsqrt_reduce_fusion, bf16[384,1024]{1,0:T(8,128)(2,1)S(1)} %copy-done.3, bf16[384,1024]{1,0:T(8,128)(2,1)S(1)} %get-tuple-element.25), kind=kOutput, calls=%fused_computation.15 | convolution fusion | flops 808845312 | bytes 4064768 | tf_op jit(solution)/shard_map/dot_general | solution.py:359
  115.2 1.3 collective-permute-start.1
  116.5 0.0 copy-done.6
  116.5 0.7 dynamic_slice.9.lam_ref
  117.2 0.1 collective-permute-done.1
  117.3 0.1 maximum_convert_fusion
  117.4 0.1 pad_add_fusion.2
  117.5 0.2 pad_add_fusion.1
  117.7 0.8 slice_bitcast_fusion.q_ref
  118.5 19.0 %all-gather.6.cloned.1.call-done = bf16[16,1,384,256]{3,2,1,0:T(8,128)(2,1)} async-done(((bf16[4,1,384,256]{3,2,1,0:T(8,128)(2,1)}), bf16[16,1,384,256]{3,2,1,0:T(8,128)(2,1)}) %all-gather.6.cloned.1.call-update) | async-done | bytes 3145744 | tf_op jit(solution)/shard_map/all_gather | solution.py:374
  137.6 36.1 %shard_map.110 = bf16[4,384,128]{2,1,0:T(8,128)(2,1)} custom-call(s32[1]{0:T(128)} %bitcast.member_ref, f32[1]{0:T(128)} %dynamic_slice.9.lam_ref, bf16[4,384,128]{2,1,0:T(8,128)(2,1)} %slice_bitcast_fusion.q_ref, bf16[4,4,384,256]{3,2,1,0:T(8,128)(2,1)} %bitcast.71, f32[1,128]{1,0:T(1,128)} %bitcast.73), custom_call_target="tpu_custom_call" | custom-call | flops 4831838208 | bytes 3145728 | tf_op jit(solution)/shard_map/pallas_call | solution.py:74
  173.7 4.7 %all-to-all-start.1 = ((bf16[4,1,384,128]{3,2,1,0:T(8,128)(2,1)}), bf16[4,1,384,128]{3,2,1,0:T(8,128)(2,1)S(1)}, u32[]{:S(2)}, u32[]{:S(2)}) async-start(bf16[4,1,384,128]{3,2,1,0:T(8,128)(2,1)} %bitcast.69), calls=%async_computation.1 | async-start | bytes 786432 | tf_op jit(solution)/shard_map/all_to_all | solution.py:383
  178.4 0.0 copy-start.5
  178.4 0.2 pad_add_fusion
  178.6 0.1 slice.38
  178.6 0.0 copy-done
  178.6 0.4 copy-done.5
  179.1 1.4 fusion.6
  180.5 13.7 %all-to-all-done.1 = bf16[4,1,384,128]{3,2,1,0:T(8,128)(2,1)S(1)} async-done(((bf16[4,1,384,128]{3,2,1,0:T(8,128)(2,1)}), bf16[4,1,384,128]{3,2,1,0:T(8,128)(2,1)S(1)}, u32[]{:S(2)}, u32[]{:S(2)}) %all-to-all-start.1) | async-done | bytes 393248 | tf_op jit(solution)/shard_map/all_to_all | solution.py:383
  194.2 0.9 copy.40
  195.2 3.4 %all-gather.4.cloned.1.call-done = bf16[1024,2048]{1,0:T(8,128)(2,1)} async-done(((bf16[1024,128]{1,0:T(8,128)(2,1)}), bf16[1024,2048]{1,0:T(8,128)(2,1)}) %all-gather.4.cloned.1.call-update) | async-done | bytes 4194320 | tf_op jit(solution)/shard_map/all_gather | solution.py:348
  198.6 4.3 %fusion.11 = f32[384,2048]{1,0:T(8,128)S(1)} fusion(bf16[1024,2048]{1,0:T(8,128)(2,1)} %all-gather.4.cloned.1.call-done, bf16[384,512]{0,1:T(8,128)(2,1)} %bitcast.68, bf16[384,512]{0,1:T(8,128)(2,1)} %bitcast.63), kind=kOutput, calls=%fused_computation.28 | convolution fusion | flops 1612185600 | bytes 8126464 | tf_op jit(solution)/shard_map/dot_general | solution.py:404
  202.9 1.0 dynamic-slice_convert_fusion
  203.9 1.3 collective-permute-start.2
  205.2 18.7 %collective-permute-done.2 = bf16[192,2048]{1,0:T(8,128)(2,1)} collective-permute-done((bf16[192,2048]{1,0:T(8,128)(2,1)}, bf16[192,2048]{1,0:T(8,128)(2,1)}, u32[]{:S(2)}, u32[]{:S(2)}) %collective-permute-start.2) | collective-permute-done | bytes 786464 | tf_op jit(solution)/shard_map/ppermute | solution.py:409
  223.9 2.2 add_convert_fusion
  (7 shorter events, 0.1 us)
Async XLA Ops:
  6.5 172.1 %copy-start = (bf16[4,128,128]{2,1,0:T(8,128)(2,1)S(1)}, bf16[4,128,128]{2,1,0:T(8,128)(2,1)}, u32[]{:S(2)}) copy-start(bf16[4,128,128]{2,1,0:T(8,128)(2,1)} %param.19) | copy-start | bytes 393220
  6.5 131.0 %all-gather.6.cloned.1.call-start = ((), (), s32[]{:S(2)}) async-start(), calls=%async_computation.3 | async-start | bytes 3932160 | tf_op jit(solution)/shard_map/all_gather | solution.py:374
  9.5 57.8 %collective-permute-start = (f32[384,1]{0,1:T(1,128)S(1)}, f32[384,1]{0,1:T(1,128)S(1)}, u32[]{:S(2)}, u32[]{:S(2)}) collective-permute-start(f32[384,1]{0,1:T(1,128)S(1)} %broadcast_in_dim.43), channel_id=1, source_target_pairs={{0,1},{1,0},{2,3},{3,2},{4,5},{5,4},{6,7},{7,6},{8,9},{9,8},{10,11... | collective-permute-start | bytes 4616 | tf_op jit(solution)/shard_map/ppermute | solution.py:350
  12.5 52.7 %copy-start.1 = (bf16[384,1024]{1,0:T(8,128)(2,1)S(1)}, bf16[384,1024]{1,0:T(8,128)(2,1)}, u32[]{:S(2)}) copy-start(bf16[384,1024]{1,0:T(8,128)(2,1)} %get-tuple-element.28.refs_4_) | copy-start | bytes 2359300
  65.2 1.3 copy-start.4
  66.5 3.6 %copy-start.2 = (bf16[384,1024]{1,0:T(8,128)(2,1)}, bf16[384,1024]{1,0:T(8,128)(2,1)S(1)}, u32[]{:S(2)}) copy-start(bf16[384,1024]{1,0:T(8,128)(2,1)S(1)} %get-tuple-element.26) | copy-start | bytes 2359300
  110.4 2.1 copy-start.3
  111.4 87.2 %all-gather.4.cloned.1.call-start = ((), (), s32[]{:S(2)}) async-start(), calls=%async_computation.2 | async-start | bytes 4456448 | tf_op jit(solution)/shard_map/all_gather | solution.py:348
  112.6 3.9 %copy-start.6 = (f32[4]{0:T(128)S(1)}, f32[4]{0:T(128)}, u32[]{:S(2)}) copy-start(f32[4]{0:T(128)} %param.17) | copy-start | bytes 52
  115.2 2.1 collective-permute-start.1
  173.7 20.5 %all-to-all-start.1 = ((bf16[4,1,384,128]{3,2,1,0:T(8,128)(2,1)}), bf16[4,1,384,128]{3,2,1,0:T(8,128)(2,1)S(1)}, u32[]{:S(2)}, u32[]{:S(2)}) async-start(bf16[4,1,384,128]{3,2,1,0:T(8,128)(2,1)} %bitcast.69), calls=%async_computation.1 | async-start | bytes 786432 | tf_op jit(solution)/shard_map/all_to_all | solution.py:383
  178.4 0.7 copy-start.5
  203.9 20.0 %collective-permute-start.2 = (bf16[192,2048]{1,0:T(8,128)(2,1)}, bf16[192,2048]{1,0:T(8,128)(2,1)}, u32[]{:S(2)}, u32[]{:S(2)}) collective-permute-start(bf16[192,2048]{1,0:T(8,128)(2,1)} %dynamic-slice_convert_fusion), channel_id=1, source_target_pairs={{0,1},{1,0},{2,3},{3,2},{4,5},{5,4},{6,7},{7,6},{8,9},{9,8},{10,11... | collective-permute-start | bytes 2359304 | tf_op jit(solution)/shard_map/ppermute | solution.py:409
Sparse Core Ops, SparseCore 0:
  111.5 26.0 all-gather.5
  139.7 58.8 all-gather.3

commit v3 on v2

--- a/solution.py
+++ b/solution.py
@@ -92,6 +92,135 @@
             flops=4 * work * vdim, bytes_accessed=kv.size * 2, transcendentals=work
         ),
     )(member, lam, q, kv, sub_gain.reshape(1, -1))
+
+
+def attend_members(hdim, lam_ref, q_ref, own_ref, gain_ref, out_ref, held, acc_ref, max_ref, send, recv):
+    outer, rows, _ = q_ref.shape
+    vdim = own_ref.shape[2] - 2 * hdim
+    sp = lax.axis_index("sp")
+    member = lax.rem(sp, 4)
+    y = lax.div(member, 2)
+    c = lax.rem(member, 2)
+    y_peer = sp + 2 - 4 * y
+    c_peer = sp + 1 - 2 * c
+    barrier = pltpu.get_barrier_semaphore()
+    for peer in (y_peer, c_peer):
+        pl.semaphore_signal(
+            barrier, 1, device_id={"sp": peer}, device_id_type=pl.DeviceIdType.MESH
+        )
+    pl.semaphore_wait(barrier, 2)
+
+    def remote(src, index, peer):
+        return pltpu.make_async_remote_copy(
+            src_ref=src,
+            dst_ref=held.at[index],
+            send_sem=send.at[index],
+            recv_sem=recv.at[index],
+            device_id={"sp": peer},
+            device_id_type=pl.DeviceIdType.MESH,
+        )
+
+    across = remote(own_ref, 1, y_peer)
+    beside = remote(own_ref, 0, c_peer)
+    onward = remote(held.at[1], 2, c_peer)
+    across.start()
+    beside.start()
+    acc_ref[...] = jnp.zeros_like(acc_ref)
+    max_ref[...] = jnp.full_like(max_ref, NEG_LARGE)
+    scale = 1.0 / math.sqrt(hdim)
+
+    def visit(ref, other):
+        shift = (member - other) * rows
+        for block in range(outer):
+            queries = (q_ref[block].astype(jnp.float32) * scale).astype(jnp.bfloat16)
+            length = (block + 1) * rows
+            keys_values = ref[: block + 1].reshape(length, 2 * hdim + vdim)
+            values = jnp.concatenate(
+                [keys_values[:, 2 * hdim :], jnp.ones((length, vdim), jnp.bfloat16)], axis=1
+            )
+            for m in range(2):
+                scores = lax.dot_general(
+                    queries[:, m * hdim : (m + 1) * hdim],
+                    keys_values[:, m * hdim : (m + 1) * hdim],
+                    (((1,), (1,)), ((), ())),
+                    preferred_element_type=jnp.float32,
+                )
+                edge = scores[:, block * rows :]
+                row = lax.broadcasted_iota(jnp.int32, edge.shape, 0)
+                col = lax.broadcasted_iota(jnp.int32, edge.shape, 1)
+                edge = jnp.where(col <= row + shift, edge, NEG_LARGE)
+                if block > 0:
+                    scores = jnp.concatenate([scores[:, : block * rows], edge], axis=1)
+                else:
+                    scores = edge
+                old_max = max_ref[block, m]
+                new_max = jnp.maximum(old_max, jnp.max(scores, axis=1, keepdims=True))
+                factor = jnp.exp(old_max - new_max)
+                expo = jnp.exp(scores - new_max[:, :1])
+                acc_ref[block, m] = acc_ref[block, m] * factor[:, :1] + jnp.dot(
+                    expo.astype(jnp.bfloat16), values, preferred_element_type=jnp.float32
+                )
+                max_ref[block, m] = new_max
+
+    visit(own_ref, member)
+
+    def arrived(j, carry):
+        @pl.when(j == 0)
+        def _():
+            beside.wait_recv()
+
+        @pl.when(j == 1)
+        def _():
+            across.wait_recv()
+            onward.start()
+
+        @pl.when(j == 2)
+        def _():
+            onward.wait_recv()
+
+        other_y = jnp.where(j >= 1, 1 - y, y)
+        other_c = jnp.where(j == 1, c, 1 - c)
+        visit(held.at[j], 2 * other_y + other_c)
+        return carry
+
+    lax.fori_loop(0, 3, arrived, 0)
+    for copy in (across, beside, onward):
+        copy.wait_send()
+    for block in range(outer):
+        first = acc_ref[block, 0]
+        second = acc_ref[block, 1]
+        mix = first[:, :vdim] / first[:, vdim:]
+        mix = mix - lam_ref[0] * (second[:, :vdim] / second[:, vdim:])
+        mean_sq = jnp.mean(mix * mix, axis=1, keepdims=True)
+        normed = mix * lax.rsqrt(mean_sq + EPSILON) * gain_ref[...]
+        out_ref[block] = normed.astype(jnp.bfloat16)
+
+
+def flash_members(q, kv, lam, sub_gain):
+    outer, rows, width = kv.shape
+    qdim = q.shape[-1]
+    vdim = width - qdim
+    vmem = pl.BlockSpec(memory_space=pltpu.VMEM)
+    work = 4 * outer * rows * outer * rows
+    return pl.pallas_call(
+        functools.partial(attend_members, qdim // 2),
+        out_shape=jax.ShapeDtypeStruct((outer, rows, vdim), jnp.bfloat16),
+        in_specs=[pl.BlockSpec(memory_space=pltpu.SMEM), vmem, vmem, vmem],
+        out_specs=vmem,
+        scratch_shapes=[
+            pltpu.VMEM((3, outer, rows, width), jnp.bfloat16),
+            pltpu.VMEM((outer, 2, rows, 2 * vdim), jnp.float32),
+            pltpu.VMEM((outer, 2, rows, 128), jnp.float32),
+            pltpu.SemaphoreType.DMA((3,)),
+            pltpu.SemaphoreType.DMA((3,)),
+        ],
+        compiler_params=pltpu.CompilerParams(
+            vmem_limit_bytes=56 * 2**20, collective_id=1, has_side_effects=True
+        ),
+        cost_estimate=pl.CostEstimate(
+            flops=4 * work * vdim, bytes_accessed=4 * kv.size * 2, transcendentals=work
+        ),
+    )(lam, q, kv, sub_gain.reshape(1, -1))
 
 
 def spread(n_sp, count, with_swap, *refs):
@@ -371,13 +500,19 @@
     by_head = by_head.reshape(outer, per_device, tok_rows, head_width)
     if outer > 1:
         by_head = lax.all_to_all(by_head, "sp", 0, 0, axis_index_groups=across)
-    kv = lax.all_gather(by_head[..., qdim:], "sp", axis=0, axis_index_groups=within)
-    member = lax.rem(sp, inner).reshape(1)
     first_head = lax.div(sp, inner) * per_device
     attended = []
-    for p in range(per_device):
-        lam = lax.dynamic_slice_in_dim(lambdas, first_head + p, 1)
-        attended.append(flash(by_head[:, p, :, :qdim], kv[:, :, p], member, lam, sub_gain))
+    if inner == 4 and per_device == 1:
+        lam = lax.dynamic_slice_in_dim(lambdas, first_head, 1)
+        attended.append(
+            flash_members(by_head[:, 0, :, :qdim], by_head[:, 0, :, qdim:], lam, sub_gain)
+        )
+    else:
+        kv = lax.all_gather(by_head[..., qdim:], "sp", axis=0, axis_index_groups=within)
+        member = lax.rem(sp, inner).reshape(1)
+        for p in range(per_device):
+            lam = lax.dynamic_slice_in_dim(lambdas, first_head + p, 1)
+            attended.append(flash(by_head[:, p, :, :qdim], kv[:, :, p], member, lam, sub_gain))
     attended = jnp.stack(attended, axis=1)
     if outer > 1:
         attended = lax.all_to_all(attended, "sp", 0, 0, axis_index_groups=across)
@@ -401,12 +536,15 @@
     branch = jnp.concatenate(
         [attended.swapaxes(0, 1).reshape(tok_rows, -1), pooled.reshape(tok_rows, -1)], axis=1
     )
-    partial = jnp.dot(branch, w_out_rows, preferred_element_type=jnp.float32)
     if n_tp == 2:
         half = tok_rows // 2
-        keep = lax.dynamic_slice_in_dim(partial, tp * half, half, 0)
-        send = lax.dynamic_slice_in_dim(partial, (1 - tp) * half, half, 0).astype(jnp.bfloat16)
-        return (keep + lax.ppermute(send, "tp", swap).astype(jnp.float32)).astype(jnp.bfloat16)
+        send = lax.dynamic_slice_in_dim(branch, (1 - tp) * half, half, 0)
+        send = jnp.dot(send, w_out_rows, preferred_element_type=jnp.float32).astype(jnp.bfloat16)
+        got = lax.ppermute(send, "tp", swap)
+        keep = lax.dynamic_slice_in_dim(branch, tp * half, half, 0)
+        keep = jnp.dot(keep, w_out_rows, preferred_element_type=jnp.float32)
+        return (keep + got.astype(jnp.float32)).astype(jnp.bfloat16)
+    partial = jnp.dot(branch, w_out_rows, preferred_element_type=jnp.float32)
     return lax.psum_scatter(partial.astype(jnp.bfloat16), "tp", scatter_dimension=0, tiled=True)
 
 

time: 233 us -> 215 us (0.923)
  blocking collectives: 33.5 us -> 0 us
  waiting for transfers between devices: 55.7 us -> 68.1 us
  starting transfers between devices: 10.3 us -> 13.3 us
    all_to_all x0 -> x1, waiting for transfers between devices: none -> 40.3 us  [local(): by_head = lax.all_to_all(by_head, 'sp', 0, 0, axis_index_groups=across)]
    all_to_all x1 -> x0, blocking collectives: 33.5 us -> none  [local(): by_head = lax.all_to_all(by_head, 'sp', 0, 0, axis_index_groups=across)]
    all_gather x1 -> x0, waiting for transfers between devices: 19 us -> none  [local(): lax.all_gather(by_head[..., qdim:], 'sp', axis=0, axis_index_groups=within)]
    all_to_all x0 -> x1, starting transfers between devices: none -> 5.07 us  [local(): by_head = lax.all_to_all(by_head, 'sp', 0, 0, axis_index_groups=across)]
    dot_general x1 -> x2, matrix products: 4.26 us -> 8.02 us  [the longest x1 4.4 us: local(): keep = jnp.dot(keep, w_out_rows, preferred_element_type=jnp.float32)]
    all_to_all x1, waiting for transfers between devices: 13.7 us -> 10.2 us  [local(): attended = lax.all_to_all(attended, 'sp', 0, 0, axis_index_groups=across)]
    all_gather x1, waiting for transfers between devices: 3.44 us -> 0.02 us  [local(): w_out_rows = lax.all_gather(w_sorted, 'sp', axis=1, tiled=True)]
  transfers between devices with their start and end apart: 6 -> 6, of which waited for: 5 -> 5; matrix products, arithmetic and copies ran while one was open for 4% -> 8% of each run, Pallas kernels for 38% -> 17%
where the time goes in v3:
time: 215 us
  Pallas kernels  90 us (42%)
  waiting for transfers between devices  68.1 us (32%)
  matrix products  17.5 us (8%)
  between operations  13.7 us (6%)
  starting transfers between devices  13.3 us (6%)
  local copies, waits for them, and re-layouts  7.27 us (3%)
  other arithmetic  5.08 us (2%)
    pallas_call x1, Pallas kernels, gather_weights(): pl.pallas_call(functools.partial(spread, n_sp, count, with_swap), out_sha...  54.5 us
    all_to_all x1, waiting for transfers between devices, local(): by_head = lax.all_to_all(by_head, 'sp', 0, 0, axis_index_groups=across)  40.3 us
    pallas_call x1, Pallas kernels, flash_members(): pl.pallas_call(functools.partial(attend_members, qdim // 2), out_shape=ja...  35.5 us
    ppermute x1, waiting for transfers between devices, local(): got = lax.ppermute(send, 'tp', swap)  16.8 us
    all_to_all x1, waiting for transfers between devices, local(): attended = lax.all_to_all(attended, 'sp', 0, 0, axis_index_groups=across)  10.2 us
    dot_general x4, matrix products, local(): jnp.dot(scaled, w, preferred_element_type=jnp.float32) * inverse  8.75 us
    all_to_all x1, starting transfers between devices, local(): by_head = lax.all_to_all(by_head, 'sp', 0, 0, axis_index_groups=across)  5.07 us
    dot_general x1, matrix products, local(): keep = jnp.dot(keep, w_out_rows, preferred_element_type=jnp.float32)  4.4 us
  transfers between devices with their start and end apart: 6, of which 5 were waited for; matrix products, arithmetic and copies ran while one was open for 8% of the time, Pallas kernels for 17%

profile of v3, /device:TPU:0, one launch (start us, length us, event | category | flops | bytes accessed | tf_op | source)
XLA Modules:
  0.0 214.9 jit_solution(7316979511020602199)
XLA Ops:
  6.5 0.0 copy-start
  6.5 0.0 all-gather.2.cloned.1.call-start
  6.5 0.7 convert_element_type.57
  7.3 1.7 copy.33
  8.9 2.2 %fusion.1 = (f32[384]{0:T(512)S(1)}, bf16[384,1024]{1,0:T(8,128)(2,1)}) fusion(bf16[384,1024]{1,0:T(8,128)(2,1)} %param.11, f32[1024]{0:T(1024)S(1)} %convert_element_type.57), kind=kLoop, calls=%fused_computation.4 | loop fusion | flops 1965696 | bytes 1578496 | tf_op jit(solution)/shard_map/reduce_sum | solution.py:467
  11.2 0.0 copy-start.1
  11.2 54.5 %shard_map.109 = (bf16[2048,512]{1,0:T(8,128)(2,1)}, bf16[2048,512]{1,0:T(8,128)(2,1)}, bf16[2048,512]{1,0:T(8,128)(2,1)}, bf16[2048,512]{1,0:T(8,128)(2,1)}, bf16[384,1024]{1,0:T(8,128)(2,1)}) custom-call(bf16[128,512]{1,0:T(8,128)(2,1)} %refs_0_.1, bf16[128,512]{1,0:T(8,128)(2,1)} %refs_1_.1, bf16[128,512]{1,0:T(8,128)(2,1)} %refs_2_.1, ...), custom_call_target="tpu_custom_call" | custom-call | flops 10000000000 | bytes 8388608 | tf_op jit(solution)/shard_map/pallas_call | solution.py:403
  65.6 0.0 all-gather.2.cloned.1.call-update
  65.7 1.6 collective-permute-start
  67.2 0.0 copy-start.7
  67.2 0.1 broadcast_bitcast_fusion.1
  67.3 0.0 copy-done.1
  67.3 1.4 broadcast_select_fusion.1
  68.7 0.0 copy-start.2
  68.7 0.6 collective-permute-done
  69.3 0.0 copy-done.7
  69.3 1.0 fusion.2
  70.3 0.2 copy.34
  70.6 2.6 %fusion.3 = bf16[384,512]{1,0:T(8,128)(2,1)S(1)} fusion(bf16[2048,512]{1,0:T(8,128)(2,1)} %get-tuple-element.21, f32[384]{0:T(512)S(1)} %rsqrt_reduce_fusion, bf16[384,1024]{1,0:T(8,128)(2,1)S(1)} %get-tuple-element.26, bf16[384,1024]{1,0:T(8,128)(2,1)S(1)} %get-tuple-element.25), kind=kOutput, calls=%fused_computation.13 | convolution fusion | flops 808845312 | bytes 4064768 | tf_op jit(solution)/shard_map/dot_general | solution.py:488
  73.1 0.2 copy.35
  73.4 0.0 copy-done.2
  73.4 2.6 %fusion.4 = bf16[384,512]{1,0:T(8,128)(2,1)S(1)} fusion(bf16[2048,512]{1,0:T(8,128)(2,1)} %get-tuple-element.22, f32[384]{0:T(512)S(1)} %rsqrt_reduce_fusion, bf16[384,1024]{1,0:T(8,128)(2,1)S(1)} %get-tuple-element.26, bf16[384,1024]{1,0:T(8,128)(2,1)S(1)} %get-tuple-element.25), kind=kOutput, calls=%fused_computation.14 | convolution fusion | flops 808845312 | bytes 4064768 | tf_op jit(solution)/shard_map/dot_general | solution.py:488
  76.0 0.2 copy.36
  76.2 0.1 maximum_bitcast_fusion
  76.3 1.5 copy.37
  77.8 0.0 copy-start.3
  77.8 5.1 %all-to-all-start = ((bf16[4,1,384,384]{3,2,1,0:T(8,128)(2,1)}), bf16[4,1,384,384]{3,2,1,0:T(8,128)(2,1)S(1)}, u32[]{:S(2)}, u32[]{:S(2)}) async-start(bf16[4,1,384,384]{3,2,1,0:T(8,128)(2,1)} %copy.37), calls=%async_computation | async-start | bytes 2359296 | tf_op jit(solution)/shard_map/all_to_all | solution.py:502
  82.9 0.1 broadcast_bitcast_fusion.2
  83.0 0.1 broadcast_bitcast_fusion.3
  83.0 0.1 broadcast_bitcast_fusion.4
  83.1 0.1 broadcast_bitcast_fusion
  83.2 0.0 copy-done.3
  83.2 0.0 copy-start.5
  83.2 2.6 %fusion.5 = bf16[384,512]{1,0:T(8,128)(2,1)S(1)} fusion(bf16[2048,512]{1,0:T(8,128)(2,1)} %get-tuple-element.23, f32[384]{0:T(512)S(1)} %rsqrt_reduce_fusion, bf16[384,1024]{1,0:T(8,128)(2,1)S(1)} %get-tuple-element.26, bf16[384,1024]{1,0:T(8,128)(2,1)S(1)} %copy-done.3), kind=kOutput, calls=%fused_computation.15 | convolution fusion | flops 808845312 | bytes 4064768 | tf_op jit(solution)/shard_map/dot_general | solution.py:488
  85.8 1.3 collective-permute-start.1
  87.1 0.0 copy-done.5
  87.1 0.7 dynamic_slice.9.lam_ref
  87.8 0.1 collective-permute-done.1
  87.9 0.1 maximum_convert_fusion
  88.0 0.1 pad_add_fusion.2
  88.1 0.2 pad_add_fusion.1
  88.3 40.3 %all-to-all-done = bf16[4,1,384,384]{3,2,1,0:T(8,128)(2,1)S(1)} async-done(((bf16[4,1,384,384]{3,2,1,0:T(8,128)(2,1)}), bf16[4,1,384,384]{3,2,1,0:T(8,128)(2,1)S(1)}, u32[]{:S(2)}, u32[]{:S(2)}) %all-to-all-start) | async-done | bytes 1179680 | tf_op jit(solution)/shard_map/all_to_all | solution.py:502
  128.6 0.8 slice_bitcast_fusion.1.q_ref
  129.5 0.9 slice_bitcast_fusion.own_ref
  130.4 35.5 %shard_map.110 = bf16[4,384,128]{2,1,0:T(8,128)(2,1)} custom-call(f32[1]{0:T(128)} %dynamic_slice.9.lam_ref, bf16[4,384,128]{2,1,0:T(8,128)(2,1)} %slice_bitcast_fusion.1.q_ref, bf16[4,384,256]{2,1,0:T(8,128)(2,1)} %slice_bitcast_fusion.own_ref, f32[1,128]{1,0:T(1,128)} %bitcast.75), custom_call_target="tpu_custom_call" | custom-call | flops 4831838208 | bytes 3145728 | tf_op jit(solution)/shard_map/pallas_call | solution.py:205
  165.9 3.5 %all-to-all-start.1 = ((bf16[4,1,384,128]{3,2,1,0:T(8,128)(2,1)}), bf16[4,1,384,128]{3,2,1,0:T(8,128)(2,1)S(1)}, u32[]{:S(2)}, u32[]{:S(2)}) async-start(bf16[4,1,384,128]{3,2,1,0:T(8,128)(2,1)} %bitcast.72), calls=%async_computation.1 | async-start | bytes 786432 | tf_op jit(solution)/shard_map/all_to_all | solution.py:518
  169.4 0.0 copy-start.4
  169.4 0.2 pad_add_fusion
  169.6 0.1 slice.38
  169.7 0.0 copy-done
  169.7 0.4 copy-done.4
  170.1 0.7 fusion.6
  170.8 0.0 copy-start.6
  170.8 10.2 %all-to-all-done.1 = bf16[4,1,384,128]{3,2,1,0:T(8,128)(2,1)S(1)} async-done(((bf16[4,1,384,128]{3,2,1,0:T(8,128)(2,1)}), bf16[4,1,384,128]{3,2,1,0:T(8,128)(2,1)S(1)}, u32[]{:S(2)}, u32[]{:S(2)}) %all-to-all-start.1) | async-done | bytes 393248 | tf_op jit(solution)/shard_map/all_to_all | solution.py:518
  181.0 0.2 copy.41
  181.3 0.0 all-gather.2.cloned.1.call-done
  181.3 0.0 copy-done.6
  181.3 3.6 %convolution_convert_fusion = bf16[192,2048]{1,0:T(8,128)(2,1)S(1)} fusion(bf16[1024,2048]{1,0:T(8,128)(2,1)} %all-gather.2.cloned.1.call-done, s32[]{:T(128)S(6)} %select_n.51, bf16[384,512]{0,1:T(8,128)(2,1)S(1)} %bitcast.70, bf16[384,512]{0,1:T(8,128)(2,1)S(1)} %bitcast.76), kind=kOutput, calls=%fused_computation | convolution fusion | flops 806486016 | bytes 5767172 | tf_op jit(solution)/shard_map/dot_general | solution.py:542
  184.9 1.9 collective-permute-start.2
  186.8 16.8 %collective-permute-done.2 = bf16[192,2048]{1,0:T(8,128)(2,1)S(1)} collective-permute-done((bf16[192,2048]{1,0:T(8,128)(2,1)S(1)}, bf16[192,2048]{1,0:T(8,128)(2,1)S(1)}, u32[]{:S(2)}, u32[]{:S(2)}) %collective-permute-start.2) | collective-permute-done | bytes 786464 | tf_op jit(solution)/shard_map/ppermute | solution.py:543
  203.6 4.4 %add_convert_fusion = bf16[192,2048]{1,0:T(8,128)(2,1)} fusion(bf16[192,2048]{1,0:T(8,128)(2,1)S(1)} %collective-permute-done.2, bf16[1024,2048]{1,0:T(8,128)(2,1)} %all-gather.2.cloned.1.call-done, s32[]{:T(128)S(6)} %select_n.50, bf16[384,512]{0,1:T(8,128)(2,1)S(1)} %bitcast.71, bf16[384,512]{0,1:T(8,128)(2,1)} %bitcast.77), kind=kOutput, calls=%fused_computation.6 | convolution fusion | flops 807272448 | bytes 6553604 | tf_op jit(solution)/shard_map/dot_general | solution.py:545
  (7 shorter events, 0.1 us)
Async XLA Ops:
  6.5 163.1 %copy-start = (bf16[4,128,128]{2,1,0:T(8,128)(2,1)S(1)}, bf16[4,128,128]{2,1,0:T(8,128)(2,1)}, u32[]{:S(2)}) copy-start(bf16[4,128,128]{2,1,0:T(8,128)(2,1)} %param.19) | copy-start | bytes 393220
  6.5 174.8 %all-gather.2.cloned.1.call-start = ((), (), s32[]{:S(2)}) async-start(), calls=%async_computation.2 | async-start | bytes 4456448 | tf_op jit(solution)/shard_map/all_gather | solution.py:477
  11.2 56.2 %copy-start.1 = (bf16[384,1024]{1,0:T(8,128)(2,1)S(1)}, bf16[384,1024]{1,0:T(8,128)(2,1)}, u32[]{:S(2)}) copy-start(bf16[384,1024]{1,0:T(8,128)(2,1)} %get-tuple-element.28.refs_4_) | copy-start | bytes 2359300
  65.7 3.6 %collective-permute-start = (f32[384,1]{0,1:T(1,128)S(1)}, f32[384,1]{0,1:T(1,128)S(1)}, u32[]{:S(2)}, u32[]{:S(2)}) collective-permute-start(f32[384,1]{0,1:T(1,128)S(1)} %broadcast_in_dim.43), channel_id=1, source_target_pairs={{0,1},{1,0},{2,3},{3,2},{4,5},{5,4},{6,7},{7,6},{8,9},{9,8},{10,11... | collective-permute-start | bytes 4616 | tf_op jit(solution)/shard_map/ppermute | solution.py:479
  67.2 2.1 copy-start.7
  68.7 4.7 %copy-start.2 = (bf16[384,1024]{1,0:T(8,128)(2,1)}, bf16[384,1024]{1,0:T(8,128)(2,1)S(1)}, u32[]{:S(2)}) copy-start(bf16[384,1024]{1,0:T(8,128)(2,1)S(1)} %get-tuple-element.25) | copy-start | bytes 2359300
  77.8 5.4 %copy-start.3 = (bf16[384,1024]{1,0:T(8,128)(2,1)S(1)}, bf16[384,1024]{1,0:T(8,128)(2,1)}, u32[]{:S(2)}) copy-start(bf16[384,1024]{1,0:T(8,128)(2,1)} %copy-done.2) | copy-start | bytes 2359300
  77.8 50.8 %all-to-all-start = ((bf16[4,1,384,384]{3,2,1,0:T(8,128)(2,1)}), bf16[4,1,384,384]{3,2,1,0:T(8,128)(2,1)S(1)}, u32[]{:S(2)}, u32[]{:S(2)}) async-start(bf16[4,1,384,384]{3,2,1,0:T(8,128)(2,1)} %copy.37), calls=%async_computation | async-start | bytes 2359296 | tf_op jit(solution)/shard_map/all_to_all | solution.py:502
  83.2 3.9 %copy-start.5 = (f32[4]{0:T(128)S(1)}, f32[4]{0:T(128)}, u32[]{:S(2)}) copy-start(f32[4]{0:T(128)} %param.17) | copy-start | bytes 52
  85.8 2.1 collective-permute-start.1
  165.9 15.1 %all-to-all-start.1 = ((bf16[4,1,384,128]{3,2,1,0:T(8,128)(2,1)}), bf16[4,1,384,128]{3,2,1,0:T(8,128)(2,1)S(1)}, u32[]{:S(2)}, u32[]{:S(2)}) async-start(bf16[4,1,384,128]{3,2,1,0:T(8,128)(2,1)} %bitcast.72), calls=%async_computation.1 | async-start | bytes 786432 | tf_op jit(solution)/shard_map/all_to_all | solution.py:518
  169.4 0.7 copy-start.4
  170.8 10.5 %copy-start.6 = (bf16[4,384,128]{1,2,0:T(8,128)(2,1)}, bf16[4,384,128]{1,2,0:T(8,128)(2,1)S(1)}, u32[]{:S(2)}) copy-start(bf16[4,384,128]{1,2,0:T(8,128)(2,1)S(1)} %fusion.6) | copy-start | bytes 1179652
  184.9 18.7 %collective-permute-start.2 = (bf16[192,2048]{1,0:T(8,128)(2,1)S(1)}, bf16[192,2048]{1,0:T(8,128)(2,1)S(1)}, u32[]{:S(2)}, u32[]{:S(2)}) collective-permute-start(bf16[192,2048]{1,0:T(8,128)(2,1)S(1)} %convolution_convert_fusion), channel_id=1, source_target_pairs={{0,1},{1,0},{2,3},{3,2},{4,5},{5,4},{6,7},{7,6},{8,9},{9,8},{10,11... | collective-permute-start | bytes 2359304 | tf_op jit(solution)/shard_map/ppermute | solution.py:543
Sparse Core Ops, SparseCore 0:
  65.8 67.5 all-gather.1
